TPU v7x, 32 devices: a whole 2x2x4 slice. The times are simulated.
32 devices in a mesh: sp: 16 (over z, y, x), tp: 2 (over core).
Axes of the slice: x: 2, y: 2, z: 4, core: 2. Of those that a mesh axis runs over, the one named last changes fastest.
Arguments:
- tokens: bfloat16 [2048, 2048], P('sp', 'tp'), may hold values from -6 to 6
- pre_gain: float32 [2048], replicated, may hold values from 0.1 to 1.9
- w_query_stick: bfloat16 [2048, 1024], P(None, 'tp'), may hold values from -0.125 to 0.125
- w_key_stick: bfloat16 [2048, 1024], P(None, 'tp'), may hold values from -0.125 to 0.125
- w_value_stick: bfloat16 [2048, 1024], P(None, 'tp'), may hold values from -2 to 2, as said below
- w_query_window: bfloat16 [2048, 1024], P(None, 'tp'), may hold values from -20 to 20, as said below
- w_key_window: bfloat16 [2048, 512], P(None, 'tp'), may hold values from -1 to 1, as said below
- w_value_window: bfloat16 [2048, 512], P(None, 'tp'), may hold values from -2 to 2, as said below
- stick_bias: float32 [16], P('tp'), may hold values from -14 to -3
- sinks: float32 [16], P('tp'), may hold values from 2 to 6
- stick_gain: float32 [1024], P('tp'), may hold values from 0.1 to 1.9
- window_gain: float32 [1024], P('tp'), may hold values from 0.1 to 1.9
- w_out_stick: bfloat16 [1024, 2048], P('tp'), may hold values from -0.125 to 0.125
- w_out_window: bfloat16 [1024, 2048], P('tp'), may hold values from -0.125 to 0.125
- post_gain: float32 [2048], replicated, may hold values from 0.1 to 1.9
Outputs:
- layer_out: bfloat16 [2048, 2048], P(('sp', 'tp'))
Inputs may be any that keep to these rules, and one draw needn't show every extreme that they name: `w_key_window`: key weights of the windowed heads. `w_query_window`: query weights of the windowed heads. `w_value_stick`: value weights of the stick-breaking heads. `w_value_window`: value weights of the windowed heads.
All inputs are finite; a program needn't handle non-finite values.
Results may differ from a plain program's by a relative error of at most 0.018.
Values may be sent and summed in bfloat16 or wider, within the bound.
A program may use at most 64 MiB of HBM per device.

v0:
```python
import functools

import jax
import jax.numpy as jnp
from jax import lax
from jax.experimental import pallas as pl
from jax.experimental.pallas import tpu as pltpu
from jax.sharding import PartitionSpec as P

HEAD_DIM = 64
GROUP = 2
WINDOW = 128
EPS = 1e-06
LOG2E = 1.4426950408889634
MESH = pl.DeviceIdType.MESH


def dot(a, b):
    return jnp.dot(a, b, preferred_element_type=jnp.float32)


def dot_t(a, b):
    return lax.dot_general(a, b, (((1,), (1,)), ((), ())), preferred_element_type=jnp.float32)


def kernel(
    n_sp,
    tokens, pre_gain_in, wqs, wks, wvs, wqw, wkw, wvw, bias_in, sinks_in, sgain_in, wgain_in, wos, wow,
    post_gain_in, out,
    pre_gain, bias, sinks, sgain, wgain, post_gain, x, bias_buf, normed, vqs, vks, vvs, vqw, vkw, vvw, vos, vow,
    kv_send, kv_all, q_pad, staged,
    kvw, kvw_prev, w_out_buf, o_send, o_recv, s_out_buf,
    sq_send, sq_recv, total_w, comb, c_send, c_recv,
    w_sem, tok_sem, x_ss, x_rs, b_ss, b_rs, kv_ss, kv_rs, f_ss, f_rs,
    p_ss, p_rs, o_ss, o_rs, sq_ss, sq_rs, c_ss, c_rs,
):
    bf = jnp.bfloat16
    f32 = jnp.float32
    s = lax.axis_index("sp")
    t = lax.axis_index("tp")
    other = 1 - t
    rows, feat_half = tokens.shape
    feats = 2 * feat_half
    half = rows // 2
    quarter = half // 2
    hd = HEAD_DIM
    heads = wqs.shape[1] // hd
    kv_heads = wkw.shape[1] // hd
    sw = wqs.shape[1]

    barrier = pltpu.get_barrier_semaphore()
    me = s * 2 + t

    def greet(k, carry):
        peer = lax.rem(me + k, 2 * n_sp)
        pl.semaphore_signal(
            barrier, inc=1, device_id={"sp": peer // 2, "tp": lax.rem(peer, 2)}, device_id_type=MESH
        )
        return carry

    lax.fori_loop(1, 2 * n_sp, greet, 0)

    loads = [
        pltpu.make_async_copy(src, dst, w_sem.at[n])
        for n, (src, dst) in enumerate(
            [(wks, vks), (wvs, vvs), (wqs, vqs), (wkw, vkw), (wvw, vvw), (wqw, vqw), (wow, vow), (wos, vos),
             (bias_in, bias), (pre_gain_in, pre_gain), (sinks_in, sinks), (sgain_in, sgain),
             (wgain_in, wgain), (post_gain_in, post_gain)]
        )
    ]
    l_ks, l_vs, l_qs, l_kw, l_vw, l_qw, l_ow, l_os, l_bias, *l_small = loads
    tok_load = pltpu.make_async_copy(tokens, x.at[t], tok_sem)
    l_bias.start()
    tok_load.start()
    for load in l_small + loads[:8]:
        load.start()

    row_id = lax.broadcasted_iota(jnp.int32, (heads, 128), 0)
    bias_rows = jnp.zeros((heads, 128), f32)
    l_bias.wait()
    for i in range(heads):
        bias_rows = jnp.where(row_id == i, bias[i] * LOG2E, bias_rows)
    bias_buf[t] = bias_rows

    for load in l_small:
        load.wait()
    tok_load.wait()
    pl.semaphore_wait(barrier, 2 * n_sp - 1)

    def to_partner(src, dst, ss, rs):
        return pltpu.make_async_remote_copy(
            src_ref=src, dst_ref=dst, send_sem=ss, recv_sem=rs,
            device_id={"sp": s, "tp": other}, device_id_type=MESH,
        )

    x_copy = to_partner(x.at[t], x.at[t], x_ss, x_rs)
    b_copy = to_partner(bias_buf.at[t], bias_buf.at[t], b_ss, b_rs)
    x_copy.start()
    b_copy.start()
    x_copy.wait_recv()

    gain = pre_gain[...].reshape(1, feats)

    def norm_step(n, carry):
        part = pl.ds(pl.multiple_of(n * 32, 32), 32)
        left = x[0, part, :].astype(f32)
        right = x[1, part, :].astype(f32)
        stats = (
            jnp.sum(left * left, axis=1, keepdims=True) + jnp.sum(right * right, axis=1, keepdims=True)
        ) * (1.0 / feats)
        inv = lax.rsqrt(stats + EPS)
        normed[part, :feat_half] = (left * inv * gain[:, :feat_half]).astype(bf)
        normed[part, feat_half:] = (right * inv * gain[:, feat_half:]).astype(bf)
        return carry

    lax.fori_loop(0, rows // 32, norm_step, 0)

    l_ks.wait()
    keys = dot(normed[...], vks[...])
    l_vs.wait()
    values = dot(normed[...], vvs[...])
    for i in range(heads):
        cols = slice(i * hd, (i + 1) * hd)
        packed = jnp.concatenate([keys[:, cols], values[:, cols]], axis=1).astype(bf)
        kv_send[i, :, :half] = packed.reshape(2, half, 2 * hd)

    def scatter(send, slots, ss, rs):
        def step(k, carry):
            i = lax.rem(k // 2 + s, heads)
            u = lax.rem(k, 2)
            chip = t * heads + i
            is_self = jnp.logical_and(chip == s, u == t)

            @pl.when(is_self)
            def _():
                pltpu.make_async_copy(send.at[i, u], slots(u), rs.at[s]).start()

            @pl.when(jnp.logical_not(is_self))
            def _():
                pltpu.make_async_remote_copy(
                    src_ref=send.at[i, u], dst_ref=slots(u), send_sem=ss.at[i, u], recv_sem=rs.at[s],
                    device_id={"sp": chip, "tp": u}, device_id_type=MESH,
                ).start()

            return carry

        lax.fori_loop(0, 2 * heads, step, 0, unroll=True)

    def scatter_done(send, slots, ss, rs):
        def step(k, carry):
            i = k // 2
            u = lax.rem(k, 2)
            chip = t * heads + i
            is_self = jnp.logical_and(chip == s, u == t)

            @pl.when(jnp.logical_not(is_self))
            def _():
                pltpu.make_async_remote_copy(
                    src_ref=send.at[i, u], dst_ref=slots(u), send_sem=ss.at[i, u], recv_sem=rs.at[s],
                    device_id={"sp": chip, "tp": u}, device_id_type=MESH,
                ).wait_send()

            return carry

        lax.fori_loop(0, 2 * heads, step, 0)

    kv_slot = lambda u: kv_all.at[s, u]

    l_qs.wait()
    queries = dot(normed[...], vqs[...])
    for i in range(heads):
        cols = slice(i * hd, (i + 1) * hd)
        for u in range(2):
            top = queries[u * half : u * half + quarter, cols]
            low = queries[u * half + quarter : (u + 1) * half, cols]
            kv_send[i, u, half:] = jnp.concatenate([top, low], axis=1).astype(bf)
    scatter(kv_send, kv_slot, kv_ss, kv_rs)

    l_kw.wait()
    kvw[:, : kv_heads * hd] = dot(normed[...], vkw[...]).astype(bf)
    l_vw.wait()
    kvw[:, kv_heads * hd :] = dot(normed[...], vvw[...]).astype(bf)
    prev_copy = lambda to: pltpu.make_async_remote_copy(
        src_ref=kvw, dst_ref=kvw_prev, send_sem=p_ss, recv_sem=p_rs,
        device_id={"sp": to, "tp": t}, device_id_type=MESH,
    )

    l_qw.wait()
    qw = dot(normed[...], vqw[...])

    def forward(k, carry):
        src = k
        pltpu.make_async_remote_copy(
            src_ref=kv_send.at[0, 0], dst_ref=kv_all.at[src, t], send_sem=kv_ss.at[0, 0],
            recv_sem=kv_rs.at[src], device_id={"sp": s, "tp": other}, device_id_type=MESH,
        ).wait_recv()
        to_partner(kv_all.at[src, t, :half], kv_all.at[src, t, :half], f_ss.at[src], f_rs.at[src]).start()
        return carry

    def forward_arrived(k, carry):
        to_partner(kv_all.at[k, other, :half], kv_all.at[k, other, :half], f_ss.at[k], f_rs.at[k]).wait_recv()
        return carry

    def forward_sent(k, carry):
        to_partner(kv_all.at[k, t, :half], kv_all.at[k, t, :half], f_ss.at[k], f_rs.at[k]).wait_send()
        return carry

    def take_q(k, carry):
        slab = kv_all[k, t, half:].astype(f32)
        zero = jnp.zeros((quarter, hd), f32)
        both = jnp.concatenate(
            [
                jnp.concatenate([slab[:, :hd], zero], axis=1),
                jnp.concatenate([slab[:, hd:], zero], axis=1),
            ],
            axis=0,
        )
        q_pad[pl.ds(pl.multiple_of(k * half, half), half), :] = both.astype(bf)
        return carry

    b_copy.wait_recv()
    head_bias = bias_buf[s // heads, pl.ds(lax.rem(s, heads), 1), :][:, :1]

    kt = 2 * rows
    chunk = 4 * half
    later = (
        lax.broadcasted_iota(jnp.int32, (kt, kt), 0) > lax.broadcasted_iota(jnp.int32, (kt, kt), 1)
    ).astype(bf)
    row = lax.broadcasted_iota(jnp.int32, (chunk, kt), 0)
    lane = lax.broadcasted_iota(jnp.int32, (chunk, kt), 1)
    q_at = (row // half) * rows + t * half + lax.rem(row, half)
    scale = LOG2E * hd**-0.5

    def tile_of(n):
        return kv_all[2 * n : 2 * n + 2, :, :half].reshape(kt, 2 * hd)

    owner = s // heads
    slot = lax.rem(s, heads)
    n_chunks = n_sp // 4

    def arrive(qc):
        lax.fori_loop(qc * 4, qc * 4 + 4, forward, 0, unroll=True)
        lax.fori_loop(qc * 4, qc * 4 + 4, take_q, 0, unroll=True)

    arrive(0)
    for qc in range(n_chunks):
        if qc + 1 < n_chunks:
            arrive(qc + 1)
        if qc + 2 == n_chunks:
            @pl.when(s < n_sp - 1)
            def _():
                prev_copy(s + 1).start()

        lax.fori_loop(qc * 4, qc * 4 + 4, forward_arrived, 0, unroll=True)
        last = 2 * qc + 1
        carry = jnp.zeros((chunk, 1), f32)
        carries = {}
        for n in range(last, -1, -1):
            low = chunk // 2 if n == last else 0
            qs = q_pad[qc * chunk + low : (qc + 1) * chunk, :]
            z = dot_t(qs, tile_of(n)) * scale + head_bias
            pos = jnp.maximum(z, 0.0)
            neg = z - pos
            soft = jnp.log2(1.0 + jnp.exp2(neg - pos))
            drop = pos + soft
            hold = neg - soft
            if n >= last - 1:
                usable = (lane + (n - 2 * qc) * kt < q_at)[low:]
                drop = jnp.where(usable, drop, 0.0)
                hold = jnp.where(usable, hold, -jnp.inf)
            suffix = dot(drop.astype(bf), later)
            staged[low:, n * kt : (n + 1) * kt] = hold - suffix
            carries[n] = carry[low:]
            step = suffix[:, :1] + drop[:, :1]
            if low:
                step = jnp.concatenate([jnp.zeros((low, 1), f32), step], axis=0)
            carry = carry + step
        acc = None
        for n in range(last - 1, -1, -1):
            weights = jnp.exp2(staged[:, n * kt : (n + 1) * kt] - carries[n]).astype(bf)
            res = dot(weights, tile_of(n))
            acc = res if acc is None else acc + res
        low = chunk // 2
        weights = jnp.exp2(staged[low:, last * kt : (last + 1) * kt] - carries[last]).astype(bf)
        tail = dot(weights, tile_of(last))
        acc = jnp.concatenate([acc[:low], acc[low:] + tail], axis=0)
        for b in range(4):
            top = acc[b * half : b * half + quarter, hd:]
            bot = acc[b * half + quarter : (b + 1) * half, hd:]
            o_send[qc * 4 + b] = jnp.concatenate([top, bot], axis=1).astype(bf)

        def give(k, carry):
            is_self = jnp.logical_and(k == s, t == owner)

            @pl.when(is_self)
            def _():
                pltpu.make_async_copy(o_send.at[k], o_recv.at[slot, t], o_rs.at[slot, t]).start()

            @pl.when(jnp.logical_not(is_self))
            def _():
                pltpu.make_async_remote_copy(
                    src_ref=o_send.at[k], dst_ref=o_recv.at[slot, t], send_sem=o_ss.at[k],
                    recv_sem=o_rs.at[slot, t], device_id={"sp": k, "tp": owner}, device_id_type=MESH,
                ).start()

            return carry

        lax.fori_loop(qc * 4, qc * 4 + 4, give, 0)

    @pl.when(s == 0)
    def _():
        kvw_prev[...] = jnp.zeros_like(kvw_prev)

    @pl.when(s > 0)
    def _():
        prev_copy(s - 1).wait_recv()

    two = 2 * rows
    r_iota = lax.broadcasted_iota(jnp.int32, (two, two), 0)
    c_iota = lax.broadcasted_iota(jnp.int32, (two, two), 1)
    dist = lax.rem(r_iota, rows) + rows - c_iota
    in_window = (dist >= 0) & (dist < WINDOW) & ((c_iota >= rows) | (s > 0))
    first_rows = lax.broadcasted_iota(jnp.int32, (two, 1), 0) < rows
    for g in range(kv_heads):
        cols = slice(g * hd, (g + 1) * hd)
        v_cols = slice((kv_heads + g) * hd, (kv_heads + g + 1) * hd)
        kk = jnp.concatenate([kvw_prev[:, cols], kvw[:, cols]], axis=0)
        vv = jnp.concatenate([kvw_prev[:, v_cols], kvw[:, v_cols]], axis=0)
        base = g * GROUP * hd
        qq = jnp.concatenate(
            [qw[:, base : base + hd], qw[:, base + hd : base + 2 * hd]], axis=0
        ).astype(bf)
        logits = jnp.where(in_window, dot_t(qq, kk) * hd**-0.5, -jnp.inf)
        sink = jnp.where(first_rows, sinks[GROUP * g], sinks[GROUP * g + 1])
        top = jnp.maximum(jnp.max(logits, axis=1, keepdims=True), sink)
        grown = jnp.exp(logits - top)
        total = jnp.sum(grown, axis=1, keepdims=True) + jnp.exp(sink - top)
        weights = (grown / total).astype(bf)
        res = dot(weights, vv)
        w_out_buf[:, base : base + 2 * hd] = jnp.concatenate([res[:rows], res[rows:]], axis=1).astype(bf)

    wf = w_out_buf[...].astype(f32)
    sq_send[0] = jnp.broadcast_to(jnp.sum(wf * wf, axis=1, keepdims=True), (rows, 128))

    sq_w = to_partner(sq_send.at[0], sq_recv.at[0], sq_ss.at[0], sq_rs.at[0])
    sq_w.start()

    l_ow.wait()
    total_w[...] = dot((wf * wgain[...].reshape(1, sw)).astype(bf), vow[...])
    sq_w.wait_recv()
    sw_cols = 2.0 * sw
    inv_w = lax.rsqrt((sq_send[0] + sq_recv[0])[:, :1] / sw_cols + EPS)

    def take_o(k, carry):
        pltpu.make_async_remote_copy(
            src_ref=o_send.at[0], dst_ref=o_recv.at[k // 2, lax.rem(k, 2)], send_sem=o_ss.at[0],
            recv_sem=o_rs.at[k // 2, lax.rem(k, 2)], device_id={"sp": s, "tp": other}, device_id_type=MESH,
        ).wait_recv()
        return carry

    lax.fori_loop(0, 2 * heads, take_o, 0)
    for j in range(heads // 2):
        for u in range(2):
            one = o_recv[2 * j, u].astype(f32)
            two_ = o_recv[2 * j + 1, u].astype(f32)
            s_out_buf[u * half : u * half + quarter, 2 * j * hd : 2 * (j + 1) * hd] = jnp.concatenate(
                [one[:, :hd], two_[:, :hd]], axis=1
            )
            s_out_buf[u * half + quarter : (u + 1) * half, 2 * j * hd : 2 * (j + 1) * hd] = jnp.concatenate(
                [one[:, hd:], two_[:, hd:]], axis=1
            )
    sf = s_out_buf[...]
    sq_send[1] = jnp.broadcast_to(jnp.sum(sf * sf, axis=1, keepdims=True), (rows, 128))
    gained = (sf * sgain[...].reshape(1, sw)).astype(bf)
    sq_s = to_partner(sq_send.at[1], sq_recv.at[1], sq_ss.at[1], sq_rs.at[1])
    sq_s.start()
    l_os.wait()
    n_cut = c_send.shape[0]
    cut = feats // n_cut
    for n in range(n_cut):
        comb[:, n * cut : (n + 1) * cut] = dot(gained, vos[:, n * cut : (n + 1) * cut])
    sq_s.wait_recv()
    inv_s = lax.rsqrt((sq_send[1] + sq_recv[1])[:, :1] / sw_cols + EPS)
    copies = []
    theirs = pl.ds(pl.multiple_of(other * half, half), half)
    mine = pl.ds(pl.multiple_of(t * half, half), half)
    for n in range(n_cut):
        cols = slice(n * cut, (n + 1) * cut)
        comb[:, cols] = comb[:, cols] * inv_s + total_w[:, cols] * inv_w
        c_send[n] = comb[theirs, cols].astype(bf)
        copy = to_partner(c_send.at[n], c_recv.at[n], c_ss.at[n], c_rs.at[n])
        copy.start()
        copies.append(copy)
    square = jnp.zeros((half, 1), f32)
    for n in range(n_cut):
        cols = slice(n * cut, (n + 1) * cut)
        copies[n].wait_recv()
        summed = (comb[mine, cols] + c_recv[n].astype(f32)).astype(bf).astype(f32)
        total_w[:half, cols] = summed
        square = square + jnp.sum(summed * summed, axis=1, keepdims=True)
    inv = lax.rsqrt(square / feats + EPS)
    out[...] = (total_w[:half, :] * inv * post_gain[...].reshape(1, feats)).astype(bf)

    x_copy.wait_send()
    b_copy.wait_send()
    scatter_done(kv_send, kv_slot, kv_ss, kv_rs)
    lax.fori_loop(0, n_sp, forward_sent, 0)

    @pl.when(s < n_sp - 1)
    def _():
        prev_copy(s + 1).wait_send()

    def gave(k, carry):
        @pl.when(jnp.logical_not(jnp.logical_and(k == s, t == owner)))
        def _():
            pltpu.make_async_remote_copy(
                src_ref=o_send.at[k], dst_ref=o_recv.at[slot, t], send_sem=o_ss.at[k],
                recv_sem=o_rs.at[slot, t], device_id={"sp": k, "tp": owner}, device_id_type=MESH,
            ).wait_send()

        return carry

    lax.fori_loop(0, n_sp, gave, 0)
    sq_w.wait_send()
    sq_s.wait_send()
    for copy in copies:
        copy.wait_send()


def one_kernel(n_sp, *args):
    tokens, pre_gain, wqs, wks, wvs, wqw, wkw, wvw, bias, sinks, sgain, wgain, wos, wow, post_gain = args
    bf = jnp.bfloat16
    f32 = jnp.float32
    rows, feat_half = tokens.shape
    feats = 2 * feat_half
    half = rows // 2
    hd = HEAD_DIM
    heads = wqs.shape[1] // hd
    sw = wqs.shape[1]
    wide = 2 * hd
    kvw_cols = wkw.shape[1] + wvw.shape[1]
    assert 2 * heads == n_sp and rows == WINDOW
    v = pltpu.VMEM
    dma = pltpu.SemaphoreType.DMA
    anywhere = pl.BlockSpec(memory_space=pl.ANY)
    vmem = pl.BlockSpec(memory_space=pltpu.VMEM)
    n_cut = 4
    scratch = [
        v(pre_gain.shape, f32), pltpu.SMEM(bias.shape, f32), pltpu.SMEM(sinks.shape, f32),
        v(sgain.shape, f32), v(wgain.shape, f32), v(post_gain.shape, f32),
        v((2, rows, feat_half), bf), v((2, heads, 128), f32), v((rows, feats), bf),
        v(wqs.shape, bf), v(wks.shape, bf), v(wvs.shape, bf), v(wqw.shape, bf), v(wkw.shape, bf),
        v(wvw.shape, bf), v(wos.shape, bf), v(wow.shape, bf),
        v((heads, 2, half + half // 2, wide), bf), v((n_sp, 2, half + half // 2, wide), bf),
        v((n_sp * half, wide), bf), v((4 * half, n_sp * rows), f32),
        v((rows, kvw_cols), bf), v((rows, kvw_cols), bf), v((rows, sw), bf),
        v((n_sp, half // 2, wide), bf), v((heads, 2, half // 2, wide), bf), v((rows, sw), f32),
        v((2, rows, 128), f32), v((2, rows, 128), f32), v((rows, feats), f32), v((rows, feats), f32),
        v((n_cut, half, feats // n_cut), bf), v((n_cut, half, feats // n_cut), bf),
        dma((14,)), dma, dma, dma, dma, dma, dma((heads, 2)), dma((n_sp,)),
        dma((n_sp,)), dma((n_sp,)), dma, dma, dma((n_sp,)), dma((heads, 2)), dma((2,)), dma((2,)),
        dma((n_cut,)), dma((n_cut,)),
    ]
    return pl.pallas_call(
        functools.partial(kernel, n_sp),
        out_shape=jax.ShapeDtypeStruct((half, feats), bf),
        in_specs=[anywhere] * len(args),
        out_specs=vmem,
        scratch_shapes=scratch,
        compiler_params=pltpu.CompilerParams(
            collective_id=0, has_side_effects=True, vmem_limit_bytes=67043328
        ),
        name="layer",
    )(*args)


def passed_along(value, axis, steps):
    count = lax.axis_size(axis)
    initial, last = (max(0, -steps), min(count, count - steps))
    return lax.ppermute(value, axis, [(source, source + steps) for source in range(initial, last)])


def rounded(values):
    return lax.optimization_barrier(values.astype(jnp.bfloat16)).astype(jnp.float32)


def norm_rows(values, gain):
    stats = jnp.mean(values * values, axis=-1, keepdims=True)
    return values * lax.rsqrt(stats + EPS) * gain


def stick_block(queries, key_pair, head_bias, key_mask, carried):
    result, logsum = carried
    head_count = queries.shape[1]
    key_rows = key_pair[0].reshape(key_pair.shape[1], head_count, HEAD_DIM)
    values = key_pair[1].reshape(key_pair.shape[1], head_count, HEAD_DIM)
    scores = jnp.einsum(
        "thd,shd->hts", queries, key_rows, preferred_element_type=jnp.float32
    ) * HEAD_DIM ** (-0.5)
    scores = scores + head_bias[:, None, None]
    usable = key_mask[None]
    log_keep = jnp.where(usable, jax.nn.log_sigmoid(-scores), 0.0)
    suffix = lax.cumsum(log_keep, axis=2, reverse=True) - log_keep
    stick_weights = jnp.where(
        usable, jnp.exp(jax.nn.log_sigmoid(scores) + suffix + logsum[:, :, None]), 0.0
    )
    stick_weights = stick_weights.astype(jnp.bfloat16)
    result = result + jnp.einsum(
        "hts,shd->htd", stick_weights, values, preferred_element_type=jnp.float32
    )
    logsum = logsum + jnp.sum(log_keep, axis=2)
    return (result, logsum)


def by_collectives(
    tokens,
    pre_gain,
    w_query_stick,
    w_key_stick,
    w_value_stick,
    w_query_window,
    w_key_window,
    w_value_window,
    stick_bias,
    sinks,
    stick_gain,
    window_gain,
    w_out_stick,
    w_out_window,
    post_gain,
):
    gathered = lax.all_gather(tokens, "tp", axis=1, tiled=True)
    normed = norm_rows(gathered.astype(jnp.float32), pre_gain).astype(jnp.bfloat16)

    def project(weight):
        return jnp.dot(normed, weight, preferred_element_type=jnp.float32).astype(jnp.bfloat16)

    tok_rows = normed.shape[0]
    dev_index = lax.axis_index("sp")
    dev_count = lax.axis_size("sp")
    query_stick = project(w_query_stick)
    stick_heads = query_stick.shape[1] // HEAD_DIM
    queries = query_stick.reshape(tok_rows, stick_heads, HEAD_DIM)
    own_pair = jnp.stack([project(w_key_stick), project(w_value_stick)])
    pair_width = own_pair.shape[2]
    positions = jnp.arange(tok_rows, dtype=jnp.int32)
    initial = (
        jnp.zeros((stick_heads, tok_rows, HEAD_DIM), jnp.float32),
        jnp.zeros((stick_heads, tok_rows), jnp.float32),
    )
    collected = own_pair[None]
    for section_index in range(dev_count.bit_length() - 1):
        arrived = passed_along(collected, "sp", 2**section_index)
        collected = jnp.concatenate([arrived, collected], axis=0)
    per_group = min(dev_count, 8)
    group_count = dev_count // per_group
    grouped = collected.reshape(group_count, per_group, 2, tok_rows, pair_width)
    grouped = grouped.transpose(0, 2, 1, 3, 4).reshape(
        group_count, 2, per_group * tok_rows, pair_width
    )
    first_source = dev_index - (dev_count - 1)
    group_starts = (first_source + jnp.arange(group_count, dtype=jnp.int32) * per_group) * tok_rows
    query_pos = dev_index * tok_rows + positions
    span_offs = jnp.arange(per_group * tok_rows, dtype=jnp.int32)

    def visit_group(carried, inputs):
        key_pair, start_pos = inputs
        key_pos = start_pos + span_offs
        key_mask = (key_pos[None, :] >= 0) & (key_pos[None, :] < query_pos[:, None])
        return (stick_block(queries, key_pair, stick_bias, key_mask, carried), None)

    (stick_sum, _), _ = lax.scan(visit_group, initial, (grouped, group_starts), reverse=True)
    stick_out = (
        stick_sum.transpose(1, 0, 2).reshape(tok_rows, stick_heads * HEAD_DIM).astype(jnp.bfloat16)
    )
    query_window = project(w_query_window)
    window_pair = jnp.stack([project(w_key_window), project(w_value_window)])
    kv_heads = window_pair.shape[2] // HEAD_DIM
    previous = passed_along(window_pair, "sp", 1)
    extended = jnp.concatenate([previous, window_pair], axis=1)
    block_count = tok_rows // WINDOW
    extended = extended.reshape(2, block_count + 1, WINDOW, kv_heads, HEAD_DIM)
    banded = jnp.concatenate([extended[:, :-1], extended[:, 1:]], axis=2)
    q_blocks = query_window.reshape(block_count, WINDOW, kv_heads, GROUP, HEAD_DIM)
    logits = jnp.einsum(
        "nqhgd,nchd->nhgqc", q_blocks, banded[0], preferred_element_type=jnp.float32
    ) * HEAD_DIM ** (-0.5)
    query_offs = jnp.arange(WINDOW, dtype=jnp.int32)[:, None]
    key_offs = jnp.arange(2 * WINDOW, dtype=jnp.int32)[None, :]
    distance = query_offs + WINDOW - key_offs
    key_pos = (
        dev_index * tok_rows
        + jnp.arange(block_count, dtype=jnp.int32)[:, None] * WINDOW
        - WINDOW
        + key_offs
    )
    usable = ((distance >= 0) & (distance < WINDOW))[None] & (key_pos >= 0)[:, None, :]
    logits = jnp.where(usable[:, None, None], logits, -jnp.inf)
    sink_logit = sinks.reshape(kv_heads, GROUP)[None, :, :, None, None]
    row_top = jnp.maximum(jnp.max(logits, axis=-1, keepdims=True), sink_logit)
    weights_exp = jnp.exp(logits - row_top)
    normalizer = jnp.sum(weights_exp, axis=-1, keepdims=True) + jnp.exp(sink_logit - row_top)
    window_weights = (weights_exp / normalizer).astype(jnp.bfloat16)
    window_sum = jnp.einsum(
        "nhgqc,nchd->nqhgd", window_weights, banded[1], preferred_element_type=jnp.float32
    )
    window_out = window_sum.reshape(tok_rows, query_window.shape[1]).astype(jnp.bfloat16)
    stick_float = stick_out.astype(jnp.float32)
    window_float = window_out.astype(jnp.float32)
    squares = lax.psum(
        (jnp.sum(stick_float * stick_float, axis=1), jnp.sum(window_float * window_float, axis=1)),
        "tp",
    )
    stick_normed = (
        stick_float * lax.rsqrt(squares[0][:, None] / (stick_gain.shape[0] * lax.axis_size("tp")) + EPS) * stick_gain
    ).astype(jnp.bfloat16)
    window_normed = (
        window_float * lax.rsqrt(squares[1][:, None] / (window_gain.shape[0] * lax.axis_size("tp")) + EPS) * window_gain
    ).astype(jnp.bfloat16)
    total = jnp.dot(stick_normed, w_out_stick, preferred_element_type=jnp.float32)
    combined = lax.psum_scatter(
        (total + jnp.dot(window_normed, w_out_window, preferred_element_type=jnp.float32)).astype(
            jnp.bfloat16
        ),
        "tp",
        scatter_dimension=0,
        tiled=True,
    ).astype(jnp.float32)
    combined = rounded(combined)
    return norm_rows(combined, post_gain).astype(jnp.bfloat16)


def solution(mesh):
    in_specs = (
        P("sp", "tp"),
        P(),
        P(None, "tp"),
        P(None, "tp"),
        P(None, "tp"),
        P(None, "tp"),
        P(None, "tp"),
        P(None, "tp"),
        P("tp"),
        P("tp"),
        P("tp"),
        P("tp"),
        P("tp", None),
        P("tp", None),
        P(),
    )
    n_sp, n_tp = mesh.shape["sp"], mesh.shape["tp"]

    def shards(*args):
        heads = args[2].shape[1] // HEAD_DIM
        if n_tp == 2 and n_tp * heads == n_sp and args[0].shape[0] == WINDOW and n_sp % 4 == 0:
            return one_kernel(n_sp, *args)
        return by_collectives(*args)

    return jax.shard_map(
        shards,
        mesh=mesh,
        in_specs=in_specs,
        out_specs=P(("sp", "tp"), None),
        check_vma=False,
    )
```

profile of v0, /device:TPU:17, one launch (start us, length us, event | category | flops | bytes accessed | tf_op | source)
XLA Modules:
  0.0 38.4 jit_solution(9723494802979893596)
XLA Ops:
  0.0 36.8 %layer.1 = bf16[64,2048]{1,0:T(8,128)(2,1)} custom-call(bf16[128,1024]{1,0:T(8,128)(2,1)} %tokens.1, f32[2048]{0:T(1024)} %pre_gain_in.1, bf16[2048,512]{1,0:T(8,128)(2,1)} %wqs.1, bf16[2048,512]{1,0:T(8,128)(2,1)} %wks.1, bf16[2048,512]{1,0:T(8,128)(2,1)} %wvs.1, bf16[2048,512]{1,0:T(8,128)(2,1)} %wqw.1, bf16[2048,256]{1,0:T(8,128)(2,1)} %wkw.1, ...), custom_call_target="tpu_custom_call" | custom-call | tf_op jit(solution)/shard_map/layer/pallas_call | solution.py:464
  36.8 1.7 %copy.17 = bf16[64,2048]{1,0:T(8,128)(2,1)} copy(bf16[64,2048]{1,0:T(8,128)(2,1)} %layer.1) | data formatting | bytes 524288
where the time goes:
time: 38.6 us; the launch traced here: 38.4 us
  Pallas kernels  36.8 us (95%)
  local copies, waits for them, and re-layouts  1.67 us (4%)
    pallas_call x1, Pallas kernels, one_kernel(): pl.pallas_call(functools.partial(kernel, n_sp), out_shape=jax.ShapeDtypeS...  36.8 us
    unnamed x1, local copies, waits for them, and re-layouts  1.67 us

commit v1 on v0

--- a/solution.py
+++ b/solution.py
@@ -15,23 +15,44 @@
 MESH = pl.DeviceIdType.MESH
 
 
+class Phases:
+    def __init__(self):
+        self.scope = None
+
+    def __call__(self, name):
+        if self.scope is not None:
+            self.scope.__exit__(None, None, None)
+            self.scope = None
+        if name:
+            self.scope = jax.named_scope(name)
+            self.scope.__enter__()
+
+
 def dot(a, b):
     return jnp.dot(a, b, preferred_element_type=jnp.float32)
 
 
 def dot_t(a, b):
     return lax.dot_general(a, b, (((1,), (1,)), ((), ())), preferred_element_type=jnp.float32)
+
+
+def chosen(at, table):
+    value = jnp.int32(table[0])
+    for n in range(1, len(table)):
+        if table[n] != table[0]:
+            value = jnp.where(at == n, jnp.int32(table[n]), value)
+    return value
 
 
 def kernel(
     n_sp,
     tokens, pre_gain_in, wqs, wks, wvs, wqw, wkw, wvw, bias_in, sinks_in, sgain_in, wgain_in, wos, wow,
     post_gain_in, out,
-    pre_gain, bias, sinks, sgain, wgain, post_gain, x, bias_buf, normed, vqs, vks, vvs, vqw, vkw, vvw, vos, vow,
-    kv_send, kv_all, q_pad, staged,
-    kvw, kvw_prev, w_out_buf, o_send, o_recv, s_out_buf,
+    pre_gain, bias, sinks, sgain, wgain, post_gain, x, bias_buf, xg, vqs, vks, vvs, vqw, vkw, vvw, vos, vow,
+    proj, kv_send, kv_all, q_pad, part, mass,
+    qw, kvw, kvw_prev, w_out_buf, o_send, o_recv, s_out_buf,
     sq_send, sq_recv, total_w, comb, c_send, c_recv,
-    w_sem, tok_sem, x_ss, x_rs, b_ss, b_rs, kv_ss, kv_rs, f_ss, f_rs,
+    w_sem, small_sem, tok_sem, x_ss, x_rs, b_ss, b_rs, kv_ss, kv_rs, f_ss, f_rs,
     p_ss, p_rs, o_ss, o_rs, sq_ss, sq_rs, c_ss, c_rs,
 ):
     bf = jnp.bfloat16
@@ -47,6 +68,21 @@
     heads = wqs.shape[1] // hd
     kv_heads = wkw.shape[1] // hd
     sw = wqs.shape[1]
+    n_chunks = n_sp // 4
+    ph = Phases()
+    ph("a_entry")
+
+    tok_load = pltpu.make_async_copy(tokens, x.at[0], tok_sem)
+    tok_load.start()
+    smalls = [
+        pltpu.make_async_copy(src, dst, small_sem.at[n])
+        for n, (src, dst) in enumerate(
+            [(bias_in, bias), (pre_gain_in, pre_gain), (sinks_in, sinks), (sgain_in, sgain),
+             (wgain_in, wgain), (post_gain_in, post_gain)]
+        )
+    ]
+    for load in smalls:
+        load.start()
 
     barrier = pltpu.get_barrier_semaphore()
     me = s * 2 + t
@@ -60,31 +96,48 @@
 
     lax.fori_loop(1, 2 * n_sp, greet, 0)
 
-    loads = [
-        pltpu.make_async_copy(src, dst, w_sem.at[n])
-        for n, (src, dst) in enumerate(
-            [(wks, vks), (wvs, vvs), (wqs, vqs), (wkw, vkw), (wvw, vvw), (wqw, vqw), (wow, vow), (wos, vos),
-             (bias_in, bias), (pre_gain_in, pre_gain), (sinks_in, sinks), (sgain_in, sgain),
-             (wgain_in, wgain), (post_gain_in, post_gain)]
-        )
-    ]
-    l_ks, l_vs, l_qs, l_kw, l_vw, l_qw, l_ow, l_os, l_bias, *l_small = loads
-    tok_load = pltpu.make_async_copy(tokens, x.at[t], tok_sem)
-    l_bias.start()
-    tok_load.start()
-    for load in l_small + loads[:8]:
-        load.start()
+    own_rows = pl.ds(pl.multiple_of(t * feat_half, feat_half), feat_half)
+    other_rows = pl.ds(pl.multiple_of(other * feat_half, feat_half), feat_half)
+    loads = {}
+    for n, (name, src, dst) in enumerate(
+        [("ks", wks, vks), ("vs", wvs, vvs), ("qs", wqs, vqs), ("kw", wkw, vkw), ("vw", wvw, vvw), ("qw", wqw, vqw)]
+    ):
+        loads[name] = [
+            pltpu.make_async_copy(src.at[own_rows], dst.at[0], w_sem.at[2 * n]),
+            pltpu.make_async_copy(src.at[other_rows], dst.at[1], w_sem.at[2 * n + 1]),
+        ]
+    l_ow = pltpu.make_async_copy(wow, vow, w_sem.at[12])
+    l_os = pltpu.make_async_copy(wos, vos, w_sem.at[13])
+
+    ph("b_tokwait")
+    tok_load.wait()
+    for load in smalls:
+        load.wait()
+    for part_of in range(2):
+        for name in ("ks", "vs", "qs"):
+            loads[name][part_of].start()
 
     row_id = lax.broadcasted_iota(jnp.int32, (heads, 128), 0)
     bias_rows = jnp.zeros((heads, 128), f32)
-    l_bias.wait()
     for i in range(heads):
         bias_rows = jnp.where(row_id == i, bias[i] * LOG2E, bias_rows)
     bias_buf[t] = bias_rows
 
-    for load in l_small:
-        load.wait()
-    tok_load.wait()
+    ph("c_gain")
+    gain = pre_gain[...].reshape(1, feats)
+    gains = [
+        jnp.where(t == 0, gain[:, :feat_half], gain[:, feat_half:]),
+        jnp.where(t == 0, gain[:, feat_half:], gain[:, :feat_half]),
+    ]
+
+    def scaled(n):
+        value = x[n].astype(f32)
+        xg[n] = (value * gains[n]).astype(bf)
+        return jnp.sum(value * value, axis=1, keepdims=True)
+
+    squares = scaled(0)
+
+    ph("d_barrier")
     pl.semaphore_wait(barrier, 2 * n_sp - 1)
 
     def to_partner(src, dst, ss, rs):
@@ -93,119 +146,102 @@
             device_id={"sp": s, "tp": other}, device_id_type=MESH,
         )
 
-    x_copy = to_partner(x.at[t], x.at[t], x_ss, x_rs)
+    x_copy = to_partner(x.at[0], x.at[1], x_ss, x_rs)
     b_copy = to_partner(bias_buf.at[t], bias_buf.at[t], b_ss, b_rs)
     x_copy.start()
     b_copy.start()
+
+    ph("e_own")
+    for n, (name, w) in enumerate([("ks", vks), ("vs", vvs), ("qs", vqs)]):
+        loads[name][0].wait()
+        proj[n] = dot(xg[0], w[0])
+    for name in ("kw", "vw", "qw"):
+        for load in loads[name]:
+            load.start()
+    ph("f_xwait")
     x_copy.wait_recv()
-
-    gain = pre_gain[...].reshape(1, feats)
-
-    def norm_step(n, carry):
-        part = pl.ds(pl.multiple_of(n * 32, 32), 32)
-        left = x[0, part, :].astype(f32)
-        right = x[1, part, :].astype(f32)
-        stats = (
-            jnp.sum(left * left, axis=1, keepdims=True) + jnp.sum(right * right, axis=1, keepdims=True)
-        ) * (1.0 / feats)
-        inv = lax.rsqrt(stats + EPS)
-        normed[part, :feat_half] = (left * inv * gain[:, :feat_half]).astype(bf)
-        normed[part, feat_half:] = (right * inv * gain[:, feat_half:]).astype(bf)
-        return carry
-
-    lax.fori_loop(0, rows // 32, norm_step, 0)
-
-    l_ks.wait()
-    keys = dot(normed[...], vks[...])
-    l_vs.wait()
-    values = dot(normed[...], vvs[...])
+    ph("g_kv")
+    inv = lax.rsqrt((squares + scaled(1)) * (1.0 / feats) + EPS)
+    loads["ks"][1].wait()
+    keys = (proj[0] + dot(xg[1], vks[1])) * inv
+    loads["vs"][1].wait()
+    values = (proj[1] + dot(xg[1], vvs[1])) * inv
     for i in range(heads):
         cols = slice(i * hd, (i + 1) * hd)
         packed = jnp.concatenate([keys[:, cols], values[:, cols]], axis=1).astype(bf)
         kv_send[i, :, :half] = packed.reshape(2, half, 2 * hd)
-
-    def scatter(send, slots, ss, rs):
-        def step(k, carry):
-            i = lax.rem(k // 2 + s, heads)
-            u = lax.rem(k, 2)
-            chip = t * heads + i
-            is_self = jnp.logical_and(chip == s, u == t)
-
-            @pl.when(is_self)
-            def _():
-                pltpu.make_async_copy(send.at[i, u], slots(u), rs.at[s]).start()
-
-            @pl.when(jnp.logical_not(is_self))
-            def _():
-                pltpu.make_async_remote_copy(
-                    src_ref=send.at[i, u], dst_ref=slots(u), send_sem=ss.at[i, u], recv_sem=rs.at[s],
-                    device_id={"sp": chip, "tp": u}, device_id_type=MESH,
-                ).start()
-
-            return carry
-
-        lax.fori_loop(0, 2 * heads, step, 0, unroll=True)
-
-    def scatter_done(send, slots, ss, rs):
-        def step(k, carry):
-            i = k // 2
-            u = lax.rem(k, 2)
-            chip = t * heads + i
-            is_self = jnp.logical_and(chip == s, u == t)
-
-            @pl.when(jnp.logical_not(is_self))
-            def _():
-                pltpu.make_async_remote_copy(
-                    src_ref=send.at[i, u], dst_ref=slots(u), send_sem=ss.at[i, u], recv_sem=rs.at[s],
-                    device_id={"sp": chip, "tp": u}, device_id_type=MESH,
-                ).wait_send()
-
-            return carry
-
-        lax.fori_loop(0, 2 * heads, step, 0)
-
-    kv_slot = lambda u: kv_all.at[s, u]
-
-    l_qs.wait()
-    queries = dot(normed[...], vqs[...])
+    ph("h_q")
+    loads["qs"][1].wait()
+    queries = (proj[2] + dot(xg[1], vqs[1])) * inv
     for i in range(heads):
         cols = slice(i * hd, (i + 1) * hd)
         for u in range(2):
             top = queries[u * half : u * half + quarter, cols]
             low = queries[u * half + quarter : (u + 1) * half, cols]
             kv_send[i, u, half:] = jnp.concatenate([top, low], axis=1).astype(bf)
-    scatter(kv_send, kv_slot, kv_ss, kv_rs)
-
-    l_kw.wait()
-    kvw[:, : kv_heads * hd] = dot(normed[...], vkw[...]).astype(bf)
-    l_vw.wait()
-    kvw[:, kv_heads * hd :] = dot(normed[...], vvw[...]).astype(bf)
+
+    ph("i_scatter")
+    zone = s // 4
+    owner = lax.rem(s, 2)
+    slot = s // 2
+
+    def dest_order(n):
+        by_zone = []
+        for z in range(n_chunks):
+            order = sorted(range(heads), key=lambda i: (SIGN * abs(i // 2 - z), i // 2, i))
+            by_zone.append(order[n])
+        return chosen(zone, by_zone)
+
+    for n in range(heads):
+        i = dest_order(n)
+        chip = 2 * i + t
+        for u in range(2):
+            is_self = jnp.logical_and(chip == s, u == t)
+
+            @pl.when(is_self)
+            def _():
+                pltpu.make_async_copy(kv_send.at[i, u], kv_all.at[s, u], kv_rs.at[s]).start()
+
+            @pl.when(jnp.logical_not(is_self))
+            def _():
+                pltpu.make_async_remote_copy(
+                    src_ref=kv_send.at[i, u], dst_ref=kv_all.at[s, u], send_sem=kv_ss.at[i, u],
+                    recv_sem=kv_rs.at[s], device_id={"sp": chip, "tp": u}, device_id_type=MESH,
+                ).start()
+
+    ph("j_wproj")
+    l_ow.start()
+    l_os.start()
+    for load in loads["kw"] + loads["vw"]:
+        load.wait()
+    kvw[:, : kv_heads * hd] = ((dot(xg[0], vkw[0]) + dot(xg[1], vkw[1])) * inv).astype(bf)
+    kvw[:, kv_heads * hd :] = ((dot(xg[0], vvw[0]) + dot(xg[1], vvw[1])) * inv).astype(bf)
     prev_copy = lambda to: pltpu.make_async_remote_copy(
         src_ref=kvw, dst_ref=kvw_prev, send_sem=p_ss, recv_sem=p_rs,
         device_id={"sp": to, "tp": t}, device_id_type=MESH,
     )
 
-    l_qw.wait()
-    qw = dot(normed[...], vqw[...])
-
-    def forward(k, carry):
-        src = k
+    @pl.when(s < n_sp - 1)
+    def _():
+        prev_copy(s + 1).start()
+
+    for load in loads["qw"]:
+        load.wait()
+    qw[...] = ((dot(xg[0], vqw[0]) + dot(xg[1], vqw[1])) * inv).astype(bf)
+
+    ph("k_misc")
+
+    def forward(src):
         pltpu.make_async_remote_copy(
             src_ref=kv_send.at[0, 0], dst_ref=kv_all.at[src, t], send_sem=kv_ss.at[0, 0],
             recv_sem=kv_rs.at[src], device_id={"sp": s, "tp": other}, device_id_type=MESH,
         ).wait_recv()
         to_partner(kv_all.at[src, t, :half], kv_all.at[src, t, :half], f_ss.at[src], f_rs.at[src]).start()
-        return carry
-
-    def forward_arrived(k, carry):
+
+    def forward_arrived(k):
         to_partner(kv_all.at[k, other, :half], kv_all.at[k, other, :half], f_ss.at[k], f_rs.at[k]).wait_recv()
-        return carry
-
-    def forward_sent(k, carry):
-        to_partner(kv_all.at[k, t, :half], kv_all.at[k, t, :half], f_ss.at[k], f_rs.at[k]).wait_send()
-        return carry
-
-    def take_q(k, carry):
+
+    def take_q(k):
         slab = kv_all[k, t, half:].astype(f32)
         zero = jnp.zeros((quarter, hd), f32)
         both = jnp.concatenate(
@@ -216,96 +252,115 @@
             axis=0,
         )
         q_pad[pl.ds(pl.multiple_of(k * half, half), half), :] = both.astype(bf)
-        return carry
 
     b_copy.wait_recv()
-    head_bias = bias_buf[s // heads, pl.ds(lax.rem(s, heads), 1), :][:, :1]
+    head_bias = bias_buf[owner, pl.ds(slot, 1), :][:, :1]
 
     kt = 2 * rows
     chunk = 4 * half
     later = (
         lax.broadcasted_iota(jnp.int32, (kt, kt), 0) > lax.broadcasted_iota(jnp.int32, (kt, kt), 1)
     ).astype(bf)
-    row = lax.broadcasted_iota(jnp.int32, (chunk, kt), 0)
-    lane = lax.broadcasted_iota(jnp.int32, (chunk, kt), 1)
-    q_at = (row // half) * rows + t * half + lax.rem(row, half)
+    low = chunk // 2
+    row = lax.broadcasted_iota(jnp.int32, (low, kt), 0)
+    lane = lax.broadcasted_iota(jnp.int32, (low, kt), 1)
+    before = lane < (row // half) * rows + t * half + lax.rem(row, half)
     scale = LOG2E * hd**-0.5
 
-    def tile_of(n):
-        return kv_all[2 * n : 2 * n + 2, :, :half].reshape(kt, 2 * hd)
-
-    owner = s // heads
-    slot = lax.rem(s, heads)
-    n_chunks = n_sp // 4
-
-    def arrive(qc):
-        lax.fori_loop(qc * 4, qc * 4 + 4, forward, 0, unroll=True)
-        lax.fori_loop(qc * 4, qc * 4 + 4, take_q, 0, unroll=True)
-
+    def tile(qs, kv, masked):
+        z = dot_t(qs, kv) * scale + head_bias
+        pos = jnp.maximum(z, 0.0)
+        neg = z - pos
+        soft = jnp.log2(1.0 + jnp.exp2(neg - pos))
+        drop = pos + soft
+        hold = neg - soft
+        if masked:
+            n = before.shape[0]
+            drop_top = jnp.where(before, drop[:n], 0.0)
+            hold_top = jnp.where(before, hold[:n], -jnp.inf)
+            drop = drop_top if n == drop.shape[0] else jnp.concatenate([drop_top, drop[n:]], axis=0)
+            hold = hold_top if n == hold.shape[0] else jnp.concatenate([hold_top, hold[n:]], axis=0)
+        suffix = dot(drop.astype(bf), later)
+        total = jnp.broadcast_to(suffix[:, :1] + drop[:, :1], (drop.shape[0], 2 * hd))
+        res = dot(jnp.exp2(hold - suffix).astype(bf), kv)
+        return res, total
+
+    def keys_of(kc, n):
+        return kv_all[pl.ds(kc * 4 + 2 * n, 2), :, :half].reshape(kt, 2 * hd)
+
+    def diagonal(c):
+        qs = q_pad[pl.ds(pl.multiple_of(c * chunk, chunk), chunk), :]
+        res1, total1 = tile(qs[low:], keys_of(c, 1), True)
+        res0, total0 = tile(qs, keys_of(c, 0), True)
+        part[c, c, :low] = res0[:low]
+        mass[c, c, :low] = total0[:low]
+        part[c, c, low:] = res1 + jnp.exp2(-total1) * res0[low:]
+        mass[c, c, low:] = total0[low:] + total1
+
+    def beyond(qc, kc):
+        qs = q_pad[pl.ds(pl.multiple_of(qc * chunk, chunk), chunk), :]
+        res1, total1 = tile(qs, keys_of(kc, 1), False)
+        res0, total0 = tile(qs, keys_of(kc, 0), False)
+        part[qc, kc] = res1 + jnp.exp2(-total1) * res0
+        mass[qc, kc] = total0 + total1
+
+    zones = []
+    for n in range(n_chunks):
+        zones.append(chosen(zone, [sorted(range(n_chunks), key=lambda c: (abs(c - z), c))[n] for z in range(n_chunks)]))
+
+    def arrive(n):
+        for b in range(4):
+            forward(zones[n] * 4 + b)
+        for b in range(4):
+            take_q(zones[n] * 4 + b)
+
+    ph("l_arrive0")
     arrive(0)
+    for n in range(n_chunks):
+        if n + 1 < n_chunks:
+            ph(f"m{n}_arrive")
+            arrive(n + 1)
+        ph(f"m{n}_fwdarr")
+        for b in range(4):
+            forward_arrived(zones[n] * 4 + b)
+        ph(f"m{n}_tiles")
+        diagonal(zones[n])
+        for m in range(n):
+            beyond(jnp.maximum(zones[n], zones[m]), jnp.minimum(zones[n], zones[m]))
+    ph("m_sum")
     for qc in range(n_chunks):
-        if qc + 1 < n_chunks:
-            arrive(qc + 1)
-        if qc + 2 == n_chunks:
-            @pl.when(s < n_sp - 1)
-            def _():
-                prev_copy(s + 1).start()
-
-        lax.fori_loop(qc * 4, qc * 4 + 4, forward_arrived, 0, unroll=True)
-        last = 2 * qc + 1
-        carry = jnp.zeros((chunk, 1), f32)
-        carries = {}
-        for n in range(last, -1, -1):
-            low = chunk // 2 if n == last else 0
-            qs = q_pad[qc * chunk + low : (qc + 1) * chunk, :]
-            z = dot_t(qs, tile_of(n)) * scale + head_bias
-            pos = jnp.maximum(z, 0.0)
-            neg = z - pos
-            soft = jnp.log2(1.0 + jnp.exp2(neg - pos))
-            drop = pos + soft
-            hold = neg - soft
-            if n >= last - 1:
-                usable = (lane + (n - 2 * qc) * kt < q_at)[low:]
-                drop = jnp.where(usable, drop, 0.0)
-                hold = jnp.where(usable, hold, -jnp.inf)
-            suffix = dot(drop.astype(bf), later)
-            staged[low:, n * kt : (n + 1) * kt] = hold - suffix
-            carries[n] = carry[low:]
-            step = suffix[:, :1] + drop[:, :1]
-            if low:
-                step = jnp.concatenate([jnp.zeros((low, 1), f32), step], axis=0)
-            carry = carry + step
-        acc = None
-        for n in range(last - 1, -1, -1):
-            weights = jnp.exp2(staged[:, n * kt : (n + 1) * kt] - carries[n]).astype(bf)
-            res = dot(weights, tile_of(n))
-            acc = res if acc is None else acc + res
-        low = chunk // 2
-        weights = jnp.exp2(staged[low:, last * kt : (last + 1) * kt] - carries[last]).astype(bf)
-        tail = dot(weights, tile_of(last))
-        acc = jnp.concatenate([acc[:low], acc[low:] + tail], axis=0)
+        acc = part[qc, qc]
+        carry = mass[qc, qc]
+        for kc in range(qc - 1, -1, -1):
+            acc = acc + jnp.exp2(-carry) * part[qc, kc]
+            if kc:
+                carry = carry + mass[qc, kc]
         for b in range(4):
             top = acc[b * half : b * half + quarter, hd:]
             bot = acc[b * half + quarter : (b + 1) * half, hd:]
             o_send[qc * 4 + b] = jnp.concatenate([top, bot], axis=1).astype(bf)
 
-        def give(k, carry):
-            is_self = jnp.logical_and(k == s, t == owner)
-
-            @pl.when(is_self)
-            def _():
-                pltpu.make_async_copy(o_send.at[k], o_recv.at[slot, t], o_rs.at[slot, t]).start()
-
-            @pl.when(jnp.logical_not(is_self))
-            def _():
-                pltpu.make_async_remote_copy(
-                    src_ref=o_send.at[k], dst_ref=o_recv.at[slot, t], send_sem=o_ss.at[k],
-                    recv_sem=o_rs.at[slot, t], device_id={"sp": k, "tp": owner}, device_id_type=MESH,
-                ).start()
-
-            return carry
-
-        lax.fori_loop(qc * 4, qc * 4 + 4, give, 0)
+    ph("m_give")
+
+    def give(k, carry):
+        is_self = jnp.logical_and(k == s, t == owner)
+
+        @pl.when(is_self)
+        def _():
+            pltpu.make_async_copy(o_send.at[k], o_recv.at[slot, t], o_rs.at[slot, t]).start()
+
+        @pl.when(jnp.logical_not(is_self))
+        def _():
+            pltpu.make_async_remote_copy(
+                src_ref=o_send.at[k], dst_ref=o_recv.at[slot, t], send_sem=o_ss.at[k],
+                recv_sem=o_rs.at[slot, t], device_id={"sp": k, "tp": owner}, device_id_type=MESH,
+            ).start()
+
+        return carry
+
+    lax.fori_loop(0, n_sp, give, 0, unroll=True)
+
+    ph("n_prev")
 
     @pl.when(s == 0)
     def _():
@@ -315,6 +370,7 @@
     def _():
         prev_copy(s - 1).wait_recv()
 
+    ph("o_window")
     two = 2 * rows
     r_iota = lax.broadcasted_iota(jnp.int32, (two, two), 0)
     c_iota = lax.broadcasted_iota(jnp.int32, (two, two), 1)
@@ -329,7 +385,7 @@
         base = g * GROUP * hd
         qq = jnp.concatenate(
             [qw[:, base : base + hd], qw[:, base + hd : base + 2 * hd]], axis=0
-        ).astype(bf)
+        )
         logits = jnp.where(in_window, dot_t(qq, kk) * hd**-0.5, -jnp.inf)
         sink = jnp.where(first_rows, sinks[GROUP * g], sinks[GROUP * g + 1])
         top = jnp.maximum(jnp.max(logits, axis=1, keepdims=True), sink)
@@ -339,6 +395,7 @@
         res = dot(weights, vv)
         w_out_buf[:, base : base + 2 * hd] = jnp.concatenate([res[:rows], res[rows:]], axis=1).astype(bf)
 
+    ph("p_sqw")
     wf = w_out_buf[...].astype(f32)
     sq_send[0] = jnp.broadcast_to(jnp.sum(wf * wf, axis=1, keepdims=True), (rows, 128))
 
@@ -347,9 +404,7 @@
 
     l_ow.wait()
     total_w[...] = dot((wf * wgain[...].reshape(1, sw)).astype(bf), vow[...])
-    sq_w.wait_recv()
-    sw_cols = 2.0 * sw
-    inv_w = lax.rsqrt((sq_send[0] + sq_recv[0])[:, :1] / sw_cols + EPS)
+    ph("r_takeo")
 
     def take_o(k, carry):
         pltpu.make_async_remote_copy(
@@ -358,7 +413,8 @@
         ).wait_recv()
         return carry
 
-    lax.fori_loop(0, 2 * heads, take_o, 0)
+    lax.fori_loop(0, 2 * heads, take_o, 0, unroll=True)
+    ph("s_sout")
     for j in range(heads // 2):
         for u in range(2):
             one = o_recv[2 * j, u].astype(f32)
@@ -371,15 +427,21 @@
             )
     sf = s_out_buf[...]
     sq_send[1] = jnp.broadcast_to(jnp.sum(sf * sf, axis=1, keepdims=True), (rows, 128))
-    gained = (sf * sgain[...].reshape(1, sw)).astype(bf)
     sq_s = to_partner(sq_send.at[1], sq_recv.at[1], sq_ss.at[1], sq_rs.at[1])
     sq_s.start()
+    ph("t_os")
+    gained = (sf * sgain[...].reshape(1, sw)).astype(bf)
     l_os.wait()
     n_cut = c_send.shape[0]
     cut = feats // n_cut
     for n in range(n_cut):
         comb[:, n * cut : (n + 1) * cut] = dot(gained, vos[:, n * cut : (n + 1) * cut])
+    sq_w.wait_recv()
+    sw_cols = 2.0 * sw
+    inv_w = lax.rsqrt((sq_send[0] + sq_recv[0])[:, :1] / sw_cols + EPS)
+    ph("u_sqwait")
     sq_s.wait_recv()
+    ph("v_csend")
     inv_s = lax.rsqrt((sq_send[1] + sq_recv[1])[:, :1] / sw_cols + EPS)
     copies = []
     theirs = pl.ds(pl.multiple_of(other * half, half), half)
@@ -391,6 +453,52 @@
         copy = to_partner(c_send.at[n], c_recv.at[n], c_ss.at[n], c_rs.at[n])
         copy.start()
         copies.append(copy)
+
+    ph("w_drain")
+    x_copy.wait_send()
+    b_copy.wait_send()
+
+    def scatter_done(k, carry):
+        i = k // 2
+        u = lax.rem(k, 2)
+        chip = 2 * i + t
+
+        @pl.when(jnp.logical_not(jnp.logical_and(chip == s, u == t)))
+        def _():
+            pltpu.make_async_remote_copy(
+                src_ref=kv_send.at[i, u], dst_ref=kv_all.at[s, u], send_sem=kv_ss.at[i, u],
+                recv_sem=kv_rs.at[s], device_id={"sp": chip, "tp": u}, device_id_type=MESH,
+            ).wait_send()
+
+        return carry
+
+    lax.fori_loop(0, 2 * heads, scatter_done, 0)
+
+    def forward_sent(k, carry):
+        to_partner(kv_all.at[k, t, :half], kv_all.at[k, t, :half], f_ss.at[k], f_rs.at[k]).wait_send()
+        return carry
+
+    lax.fori_loop(0, n_sp, forward_sent, 0)
+
+    @pl.when(s < n_sp - 1)
+    def _():
+        prev_copy(s + 1).wait_send()
+
+    def gave(k, carry):
+        @pl.when(jnp.logical_not(jnp.logical_and(k == s, t == owner)))
+        def _():
+            pltpu.make_async_remote_copy(
+                src_ref=o_send.at[k], dst_ref=o_recv.at[slot, t], send_sem=o_ss.at[k],
+                recv_sem=o_rs.at[slot, t], device_id={"sp": k, "tp": owner}, device_id_type=MESH,
+            ).wait_send()
+
+        return carry
+
+    lax.fori_loop(0, n_sp, gave, 0)
+    sq_w.wait_send()
+    sq_s.wait_send()
+
+    ph("x_crecv")
     square = jnp.zeros((half, 1), f32)
     for n in range(n_cut):
         cols = slice(n * cut, (n + 1) * cut)
@@ -398,33 +506,15 @@
         summed = (comb[mine, cols] + c_recv[n].astype(f32)).astype(bf).astype(f32)
         total_w[:half, cols] = summed
         square = square + jnp.sum(summed * summed, axis=1, keepdims=True)
+    ph("y_out")
     inv = lax.rsqrt(square / feats + EPS)
     out[...] = (total_w[:half, :] * inv * post_gain[...].reshape(1, feats)).astype(bf)
-
-    x_copy.wait_send()
-    b_copy.wait_send()
-    scatter_done(kv_send, kv_slot, kv_ss, kv_rs)
-    lax.fori_loop(0, n_sp, forward_sent, 0)
-
-    @pl.when(s < n_sp - 1)
-    def _():
-        prev_copy(s + 1).wait_send()
-
-    def gave(k, carry):
-        @pl.when(jnp.logical_not(jnp.logical_and(k == s, t == owner)))
-        def _():
-            pltpu.make_async_remote_copy(
-                src_ref=o_send.at[k], dst_ref=o_recv.at[slot, t], send_sem=o_ss.at[k],
-                recv_sem=o_rs.at[slot, t], device_id={"sp": k, "tp": owner}, device_id_type=MESH,
-            ).wait_send()
-
-        return carry
-
-    lax.fori_loop(0, n_sp, gave, 0)
-    sq_w.wait_send()
-    sq_s.wait_send()
     for copy in copies:
         copy.wait_send()
+    ph(None)
+
+
+SIGN = -1
 
 
 def one_kernel(n_sp, *args):
@@ -439,39 +529,42 @@
     sw = wqs.shape[1]
     wide = 2 * hd
     kvw_cols = wkw.shape[1] + wvw.shape[1]
+    n_chunks = n_sp // 4
     assert 2 * heads == n_sp and rows == WINDOW
     v = pltpu.VMEM
     dma = pltpu.SemaphoreType.DMA
     anywhere = pl.BlockSpec(memory_space=pl.ANY)
     vmem = pl.BlockSpec(memory_space=pltpu.VMEM)
     n_cut = 4
+    split = lambda w: v((2, w.shape[0] // 2, w.shape[1]), bf)
     scratch = [
         v(pre_gain.shape, f32), pltpu.SMEM(bias.shape, f32), pltpu.SMEM(sinks.shape, f32),
         v(sgain.shape, f32), v(wgain.shape, f32), v(post_gain.shape, f32),
-        v((2, rows, feat_half), bf), v((2, heads, 128), f32), v((rows, feats), bf),
-        v(wqs.shape, bf), v(wks.shape, bf), v(wvs.shape, bf), v(wqw.shape, bf), v(wkw.shape, bf),
-        v(wvw.shape, bf), v(wos.shape, bf), v(wow.shape, bf),
+        v((2, rows, feat_half), bf), v((2, heads, 128), f32), v((2, rows, feat_half), bf),
+        split(wqs), split(wks), split(wvs), split(wqw), split(wkw), split(wvw), v(wos.shape, bf), v(wow.shape, bf),
+        v((3, rows, sw), f32),
         v((heads, 2, half + half // 2, wide), bf), v((n_sp, 2, half + half // 2, wide), bf),
-        v((n_sp * half, wide), bf), v((4 * half, n_sp * rows), f32),
-        v((rows, kvw_cols), bf), v((rows, kvw_cols), bf), v((rows, sw), bf),
+        v((n_sp * half, wide), bf),
+        v((n_chunks, n_chunks, 4 * half, wide), f32), v((n_chunks, n_chunks, 4 * half, wide), f32),
+        v((rows, sw), bf), v((rows, kvw_cols), bf), v((rows, kvw_cols), bf), v((rows, sw), bf),
         v((n_sp, half // 2, wide), bf), v((heads, 2, half // 2, wide), bf), v((rows, sw), f32),
         v((2, rows, 128), f32), v((2, rows, 128), f32), v((rows, feats), f32), v((rows, feats), f32),
         v((n_cut, half, feats // n_cut), bf), v((n_cut, half, feats // n_cut), bf),
-        dma((14,)), dma, dma, dma, dma, dma, dma((heads, 2)), dma((n_sp,)),
+        dma((14,)), dma((6,)), dma, dma, dma, dma, dma, dma((heads, 2)), dma((n_sp,)),
         dma((n_sp,)), dma((n_sp,)), dma, dma, dma((n_sp,)), dma((heads, 2)), dma((2,)), dma((2,)),
         dma((n_cut,)), dma((n_cut,)),
     ]
     return pl.pallas_call(
         functools.partial(kernel, n_sp),
-        out_shape=jax.ShapeDtypeStruct((half, feats), bf),
+        out_shape=pltpu.VMEM((half, feats), bf),
         in_specs=[anywhere] * len(args),
         out_specs=vmem,
         scratch_shapes=scratch,
         compiler_params=pltpu.CompilerParams(
-            collective_id=0, has_side_effects=True, vmem_limit_bytes=67043328
+            collective_id=0, has_side_effects=True, vmem_limit_bytes=60 * 1024 * 1024
         ),
         name="layer",
-    )(*args)
+    )(*[pltpu.with_memory_space_constraint(a, pltpu.HBM) for a in args])
 
 
 def passed_along(value, axis, steps):

time: 38.6 us -> 33.8 us (0.88)
  the two profiles are of different devices: /device:TPU:17 before, /device:TPU:0 now
where the time goes in v1:
time: 33.8 us; the launch traced here: 33.7 us
  Pallas kernels  33 us (98%)
  local copies, waits for them, and re-layouts  0.71 us (2%)
    pallas_call x1, Pallas kernels, one_kernel(): pl.pallas_call(functools.partial(kernel, n_sp), out_shape=pltpu.VMEM((hal...  33 us
    unnamed x1, local copies, waits for them, and re-layouts  0.71 us

profile of v1, /device:TPU:0, one launch (start us, length us, event | category | flops | bytes accessed | tf_op | source)
XLA Modules:
  0.0 33.7 jit_solution(313091958572532485)
XLA Ops:
  0.0 33.0 %layer.1 = bf16[64,2048]{1,0:T(8,128)(2,1)S(1)} custom-call(bf16[128,1024]{1,0:T(8,128)(2,1)} %tokens.1, f32[2048]{0:T(1024)} %pre_gain_in.1, bf16[2048,512]{1,0:T(8,128)(2,1)} %wqs.1, bf16[2048,512]{1,0:T(8,128)(2,1)} %wks.1, bf16[2048,512]{1,0:T(8,128)(2,1)} %wvs.1, bf16[2048,512]{1,0:T(8,128)(2,1)} %wqw.1, bf16[2048,256]{1,0:T(8,128)(2,1)} %wkw.1, ...), custom_call_target="tpu_custom_call" | custom-call | tf_op jit(solution)/shard_map/layer/pallas_call | solution.py:557
  33.0 0.7 %copy.17 = bf16[64,2048]{1,0:T(8,128)(2,1)} copy(bf16[64,2048]{1,0:T(8,128)(2,1)S(1)} %layer.1) | data formatting | bytes 524288

commit v2 on v1

--- a/solution.py
+++ b/solution.py
@@ -44,6 +44,14 @@
     return value
 
 
+def zone_order(z, count):
+    return sorted(range(count), key=lambda c: (2 * c // count != 2 * z // count, abs(c - z)))
+
+
+def send_order(z, count):
+    return sorted(range(count), key=lambda c: (abs(c - z), 2 * c // count != 2 * z // count))
+
+
 def kernel(
     n_sp,
     tokens, pre_gain_in, wqs, wks, wvs, wqw, wkw, wvw, bias_in, sinks_in, sgain_in, wgain_in, wos, wow,
@@ -51,9 +59,9 @@
     pre_gain, bias, sinks, sgain, wgain, post_gain, x, bias_buf, xg, vqs, vks, vvs, vqw, vkw, vvw, vos, vow,
     proj, kv_send, kv_all, q_pad, part, mass,
     qw, kvw, kvw_prev, w_out_buf, o_send, o_recv, s_out_buf,
-    sq_send, sq_recv, total_w, comb, c_send, c_recv,
+    sq_send, sq_recv, total_w, comb, c_send, c_recv, wc_send, wc_recv,
     w_sem, small_sem, tok_sem, x_ss, x_rs, b_ss, b_rs, kv_ss, kv_rs, f_ss, f_rs,
-    p_ss, p_rs, o_ss, o_rs, sq_ss, sq_rs, c_ss, c_rs,
+    p_ss, p_rs, o_ss, o_rs, sq_ss, sq_rs, c_ss, c_rs, wc_ss, wc_rs, hello, all_in,
 ):
     bf = jnp.bfloat16
     f32 = jnp.float32
@@ -85,16 +93,19 @@
         load.start()
 
     barrier = pltpu.get_barrier_semaphore()
-    me = s * 2 + t
+    partner = {"sp": s, "tp": other}
+
+    @pl.when(t == 0)
+    def _():
+        pl.semaphore_signal(barrier, inc=1, device_id=partner, device_id_type=MESH)
 
     def greet(k, carry):
-        peer = lax.rem(me + k, 2 * n_sp)
         pl.semaphore_signal(
-            barrier, inc=1, device_id={"sp": peer // 2, "tp": lax.rem(peer, 2)}, device_id_type=MESH
+            barrier, inc=1, device_id={"sp": lax.rem(s + k, n_sp), "tp": 0}, device_id_type=MESH
         )
         return carry
 
-    lax.fori_loop(1, 2 * n_sp, greet, 0)
+    lax.fori_loop(1, n_sp, greet, 0, unroll=True)
 
     own_rows = pl.ds(pl.multiple_of(t * feat_half, feat_half), feat_half)
     other_rows = pl.ds(pl.multiple_of(other * feat_half, feat_half), feat_half)
@@ -109,13 +120,32 @@
     l_ow = pltpu.make_async_copy(wow, vow, w_sem.at[12])
     l_os = pltpu.make_async_copy(wos, vos, w_sem.at[13])
 
-    ph("b_tokwait")
-    tok_load.wait()
-    for load in smalls:
-        load.wait()
     for part_of in range(2):
         for name in ("ks", "vs", "qs"):
             loads[name][part_of].start()
+    ph("b_hello")
+
+    @pl.when(t == 1)
+    def _():
+        pl.semaphore_wait(barrier, 1)
+        pl.semaphore_signal(hello, inc=1, device_id=partner, device_id_type=MESH)
+
+    @pl.when(t == 0)
+    def _():
+        pl.semaphore_wait(hello, 1)
+
+    def to_partner(src, dst, ss, rs):
+        return pltpu.make_async_remote_copy(
+            src_ref=src, dst_ref=dst, send_sem=ss, recv_sem=rs,
+            device_id={"sp": s, "tp": other}, device_id_type=MESH,
+        )
+
+    ph("b_tokwait")
+    tok_load.wait()
+    x_copy = to_partner(x.at[0], x.at[1], x_ss, x_rs)
+    x_copy.start()
+    for load in smalls:
+        load.wait()
 
     row_id = lax.broadcasted_iota(jnp.int32, (heads, 128), 0)
     bias_rows = jnp.zeros((heads, 128), f32)
@@ -137,18 +167,7 @@
 
     squares = scaled(0)
 
-    ph("d_barrier")
-    pl.semaphore_wait(barrier, 2 * n_sp - 1)
-
-    def to_partner(src, dst, ss, rs):
-        return pltpu.make_async_remote_copy(
-            src_ref=src, dst_ref=dst, send_sem=ss, recv_sem=rs,
-            device_id={"sp": s, "tp": other}, device_id_type=MESH,
-        )
-
-    x_copy = to_partner(x.at[0], x.at[1], x_ss, x_rs)
     b_copy = to_partner(bias_buf.at[t], bias_buf.at[t], b_ss, b_rs)
-    x_copy.start()
     b_copy.start()
 
     ph("e_own")
@@ -160,19 +179,17 @@
             load.start()
     ph("f_xwait")
     x_copy.wait_recv()
-    ph("g_kv")
+    ph("g_kvq")
+    for name in ("ks", "vs", "qs"):
+        loads[name][1].wait()
     inv = lax.rsqrt((squares + scaled(1)) * (1.0 / feats) + EPS)
-    loads["ks"][1].wait()
     keys = (proj[0] + dot(xg[1], vks[1])) * inv
-    loads["vs"][1].wait()
     values = (proj[1] + dot(xg[1], vvs[1])) * inv
     for i in range(heads):
         cols = slice(i * hd, (i + 1) * hd)
         packed = jnp.concatenate([keys[:, cols], values[:, cols]], axis=1).astype(bf)
         kv_send[i, :, :half] = packed.reshape(2, half, 2 * hd)
-    ph("h_q")
-    loads["qs"][1].wait()
-    queries = (proj[2] + dot(xg[1], vqs[1])) * inv
+    queries = (proj[2] + dot(xg[1], vqs[1])) * (inv * (LOG2E * hd**-0.5))
     for i in range(heads):
         cols = slice(i * hd, (i + 1) * hd)
         for u in range(2):
@@ -180,6 +197,17 @@
             low = queries[u * half + quarter : (u + 1) * half, cols]
             kv_send[i, u, half:] = jnp.concatenate([top, low], axis=1).astype(bf)
 
+    ph("h_barrier")
+
+    @pl.when(t == 0)
+    def _():
+        pl.semaphore_wait(barrier, 2 * (n_sp - 1))
+        pl.semaphore_signal(all_in, inc=1, device_id=partner, device_id_type=MESH)
+
+    @pl.when(t == 1)
+    def _():
+        pl.semaphore_wait(all_in, 1)
+
     ph("i_scatter")
     zone = s // 4
     owner = lax.rem(s, 2)
@@ -188,7 +216,7 @@
     def dest_order(n):
         by_zone = []
         for z in range(n_chunks):
-            order = sorted(range(heads), key=lambda i: (SIGN * abs(i // 2 - z), i // 2, i))
+            order = [2 * c + y for c in send_order(z, n_chunks) for y in range(2)]
             by_zone.append(order[n])
         return chosen(zone, by_zone)
 
@@ -257,108 +285,133 @@
     head_bias = bias_buf[owner, pl.ds(slot, 1), :][:, :1]
 
     kt = 2 * rows
-    chunk = 4 * half
     later = (
         lax.broadcasted_iota(jnp.int32, (kt, kt), 0) > lax.broadcasted_iota(jnp.int32, (kt, kt), 1)
     ).astype(bf)
-    low = chunk // 2
-    row = lax.broadcasted_iota(jnp.int32, (low, kt), 0)
-    lane = lax.broadcasted_iota(jnp.int32, (low, kt), 1)
+    row = lax.broadcasted_iota(jnp.int32, (rows, kt), 0)
+    lane = lax.broadcasted_iota(jnp.int32, (rows, kt), 1)
     before = lane < (row // half) * rows + t * half + lax.rem(row, half)
-    scale = LOG2E * hd**-0.5
-
-    def tile(qs, kv, masked):
-        z = dot_t(qs, kv) * scale + head_bias
-        pos = jnp.maximum(z, 0.0)
-        neg = z - pos
-        soft = jnp.log2(1.0 + jnp.exp2(neg - pos))
-        drop = pos + soft
-        hold = neg - soft
-        if masked:
-            n = before.shape[0]
-            drop_top = jnp.where(before, drop[:n], 0.0)
-            hold_top = jnp.where(before, hold[:n], -jnp.inf)
-            drop = drop_top if n == drop.shape[0] else jnp.concatenate([drop_top, drop[n:]], axis=0)
-            hold = hold_top if n == hold.shape[0] else jnp.concatenate([hold_top, hold[n:]], axis=0)
-        suffix = dot(drop.astype(bf), later)
-        total = jnp.broadcast_to(suffix[:, :1] + drop[:, :1], (drop.shape[0], 2 * hd))
-        res = dot(jnp.exp2(hold - suffix).astype(bf), kv)
-        return res, total
-
-    def keys_of(kc, n):
-        return kv_all[pl.ds(kc * 4 + 2 * n, 2), :, :half].reshape(kt, 2 * hd)
-
-    def diagonal(c):
-        qs = q_pad[pl.ds(pl.multiple_of(c * chunk, chunk), chunk), :]
-        res1, total1 = tile(qs[low:], keys_of(c, 1), True)
-        res0, total0 = tile(qs, keys_of(c, 0), True)
-        part[c, c, :low] = res0[:low]
-        mass[c, c, :low] = total0[:low]
-        part[c, c, low:] = res1 + jnp.exp2(-total1) * res0[low:]
-        mass[c, c, low:] = total0[low:] + total1
-
-    def beyond(qc, kc):
-        qs = q_pad[pl.ds(pl.multiple_of(qc * chunk, chunk), chunk), :]
-        res1, total1 = tile(qs, keys_of(kc, 1), False)
-        res0, total0 = tile(qs, keys_of(kc, 0), False)
-        part[qc, kc] = res1 + jnp.exp2(-total1) * res0
-        mass[qc, kc] = total0 + total1
-
-    zones = []
-    for n in range(n_chunks):
-        zones.append(chosen(zone, [sorted(range(n_chunks), key=lambda c: (abs(c - z), c))[n] for z in range(n_chunks)]))
+
+    def weigh(tiles):
+        drops, holds = [], []
+        for qs, kv, masked in tiles:
+            z = dot_t(qs, kv) + head_bias
+            pos = jnp.maximum(z, 0.0)
+            drop = pos + jnp.log2(1.0 + jnp.exp2(z - pos - pos))
+            hold = z - drop
+            if masked:
+                drop_top = jnp.where(before, drop[:rows], 0.0)
+                hold_top = jnp.where(before, hold[:rows], -jnp.inf)
+                if drop.shape[0] == rows:
+                    drop, hold = drop_top, hold_top
+                else:
+                    drop = jnp.concatenate([drop_top, drop[rows:]], axis=0)
+                    hold = jnp.concatenate([hold_top, hold[rows:]], axis=0)
+            drops.append(drop)
+            holds.append(hold)
+        suffixes = [dot(drop.astype(bf), later) for drop in drops]
+        results = []
+        for (_, kv, _), drop, hold, suffix in zip(tiles, drops, holds, suffixes):
+            total = jnp.broadcast_to(suffix[:, :1] + drop[:, :1], (drop.shape[0], 2 * hd))
+            results.append((dot(jnp.exp2(hold - suffix).astype(bf), kv), total))
+        return results
+
+    def keys_of(g):
+        return kv_all[pl.ds(2 * g, 2), :, :half].reshape(kt, 2 * hd)
+
+    def queries_of(g, count):
+        return q_pad[pl.ds(pl.multiple_of(g * rows, rows), count * rows), :]
+
+    def take_zone(c, others):
+        places = [(2 * c + 1, 2 * c + 1, 1, True), (2 * c, 2 * c, 2, True)]
+        for e in others:
+            qc, kc = jnp.maximum(c, e), jnp.minimum(c, e)
+            places += [(2 * qc, 2 * kc, 2, False), (2 * qc, 2 * kc + 1, 2, False)]
+        step = 4
+        for n in range(0, len(places), step):
+            some = places[n : n + step]
+            results = weigh([(queries_of(q, count), keys_of(g), masked) for q, g, count, masked in some])
+            for (q, g, count, _), (res, total) in zip(some, results):
+                part[g, pl.ds(q, count)] = res.reshape(count, rows, 2 * hd)
+                mass[g, pl.ds(q, count)] = total.reshape(count, rows, 2 * hd)
+
+    def finish(g):
+        def add(j, carry):
+            acc, passed = carry
+            k = g - j
+            return acc + jnp.exp2(-passed) * part[k, g], passed + mass[k, g]
+
+        acc, _ = lax.fori_loop(1, g + 1, add, (part[g, g], mass[g, g]))
+        for b in range(2):
+            top = acc[b * half : b * half + quarter, hd:]
+            bot = acc[b * half + quarter : (b + 1) * half, hd:]
+            o_send[2 * g + b] = jnp.concatenate([top, bot], axis=1).astype(bf)
+        for b in range(2):
+            k = 2 * g + b
+            is_self = jnp.logical_and(k == s, t == owner)
+
+            @pl.when(is_self)
+            def _():
+                pltpu.make_async_copy(o_send.at[k], o_recv.at[slot, t], o_rs.at[slot, t]).start()
+
+            @pl.when(jnp.logical_not(is_self))
+            def _():
+                pltpu.make_async_remote_copy(
+                    src_ref=o_send.at[k], dst_ref=o_recv.at[slot, t], send_sem=o_ss.at[k],
+                    recv_sem=o_rs.at[slot, t], device_id={"sp": k, "tp": owner}, device_id_type=MESH,
+                ).start()
+
+    def finish_range(lo, hi):
+        def step(g, carry):
+            finish(g)
+            return carry
+
+        lax.fori_loop(lo, hi, step, 0)
+
+    takes = [zone_order(z, n_chunks) for z in range(n_chunks)]
+    units = []
+    for z in range(n_chunks):
+        mine_units = [[2 * c, 2 * c + 1] for c in takes[z]]
+        units.append(mine_units)
+    n_units = len(units[0])
+    ends = []
+    for z in range(n_chunks):
+        seen, done, spans = set(), 0, []
+        for unit in units[z]:
+            seen |= set(unit)
+            upto = done
+            while upto in seen:
+                upto += 1
+            spans.append((done, upto))
+            done = upto
+        ends.append(spans)
+    group = [[chosen(zone, [units[z][n][m] for z in range(n_chunks)]) for m in range(len(units[0][n]))] for n in range(n_units)]
 
     def arrive(n):
-        for b in range(4):
-            forward(zones[n] * 4 + b)
-        for b in range(4):
-            take_q(zones[n] * 4 + b)
+        for g in group[n]:
+            for b in range(2):
+                forward(2 * g + b)
+        for g in group[n]:
+            for b in range(2):
+                take_q(2 * g + b)
+
+    def arrived(n):
+        for g in group[n]:
+            for b in range(2):
+                forward_arrived(2 * g + b)
 
     ph("l_arrive0")
     arrive(0)
-    for n in range(n_chunks):
-        if n + 1 < n_chunks:
+    for n in range(n_units):
+        if n + 1 < n_units:
             ph(f"m{n}_arrive")
             arrive(n + 1)
         ph(f"m{n}_fwdarr")
-        for b in range(4):
-            forward_arrived(zones[n] * 4 + b)
+        arrived(n)
         ph(f"m{n}_tiles")
-        diagonal(zones[n])
-        for m in range(n):
-            beyond(jnp.maximum(zones[n], zones[m]), jnp.minimum(zones[n], zones[m]))
-    ph("m_sum")
-    for qc in range(n_chunks):
-        acc = part[qc, qc]
-        carry = mass[qc, qc]
-        for kc in range(qc - 1, -1, -1):
-            acc = acc + jnp.exp2(-carry) * part[qc, kc]
-            if kc:
-                carry = carry + mass[qc, kc]
-        for b in range(4):
-            top = acc[b * half : b * half + quarter, hd:]
-            bot = acc[b * half + quarter : (b + 1) * half, hd:]
-            o_send[qc * 4 + b] = jnp.concatenate([top, bot], axis=1).astype(bf)
-
-    ph("m_give")
-
-    def give(k, carry):
-        is_self = jnp.logical_and(k == s, t == owner)
-
-        @pl.when(is_self)
-        def _():
-            pltpu.make_async_copy(o_send.at[k], o_recv.at[slot, t], o_rs.at[slot, t]).start()
-
-        @pl.when(jnp.logical_not(is_self))
-        def _():
-            pltpu.make_async_remote_copy(
-                src_ref=o_send.at[k], dst_ref=o_recv.at[slot, t], send_sem=o_ss.at[k],
-                recv_sem=o_rs.at[slot, t], device_id={"sp": k, "tp": owner}, device_id_type=MESH,
-            ).start()
-
-        return carry
-
-    lax.fori_loop(0, n_sp, give, 0, unroll=True)
+        take_zone(group[n][0] // 2, [group[m][0] // 2 for m in range(n)])
+        ph(f"m{n}_finish")
+        finish_range(chosen(zone, [ends[z][n][0] for z in range(n_chunks)]), chosen(zone, [ends[z][n][1] for z in range(n_chunks)]))
 
     ph("n_prev")
 
@@ -396,14 +449,32 @@
         w_out_buf[:, base : base + 2 * hd] = jnp.concatenate([res[:rows], res[rows:]], axis=1).astype(bf)
 
     ph("p_sqw")
+    theirs = pl.ds(pl.multiple_of(other * half, half), half)
+    mine = pl.ds(pl.multiple_of(t * half, half), half)
+    n_cut = c_send.shape[0]
+    cut = feats // n_cut
+
+    def squares_to_partner(n, squared):
+        sq_send[n] = jnp.broadcast_to(jnp.sum(squared, axis=1, keepdims=True), (rows, 128))
+        copy = to_partner(sq_send.at[n, theirs], sq_recv.at[n], sq_ss.at[n], sq_rs.at[n])
+        copy.start()
+        return copy
+
+    def halves_to_partner(left, weights, total, send, recv, ss, rs):
+        copies = []
+        for n in range(n_cut):
+            cols = slice(n * cut, (n + 1) * cut)
+            total[:, cols] = dot(left, weights[:, cols])
+            send[n] = total[theirs, cols].astype(bf)
+            copy = to_partner(send.at[n], recv.at[n], ss.at[n], rs.at[n])
+            copy.start()
+            copies.append(copy)
+        return copies
+
     wf = w_out_buf[...].astype(f32)
-    sq_send[0] = jnp.broadcast_to(jnp.sum(wf * wf, axis=1, keepdims=True), (rows, 128))
-
-    sq_w = to_partner(sq_send.at[0], sq_recv.at[0], sq_ss.at[0], sq_rs.at[0])
-    sq_w.start()
-
+    sq_w = squares_to_partner(0, wf * wf)
     l_ow.wait()
-    total_w[...] = dot((wf * wgain[...].reshape(1, sw)).astype(bf), vow[...])
+    w_copies = halves_to_partner((wf * wgain[...].reshape(1, sw)).astype(bf), vow, total_w, wc_send, wc_recv, wc_ss, wc_rs)
     ph("r_takeo")
 
     def take_o(k, carry):
@@ -426,33 +497,18 @@
                 [one[:, hd:], two_[:, hd:]], axis=1
             )
     sf = s_out_buf[...]
-    sq_send[1] = jnp.broadcast_to(jnp.sum(sf * sf, axis=1, keepdims=True), (rows, 128))
-    sq_s = to_partner(sq_send.at[1], sq_recv.at[1], sq_ss.at[1], sq_rs.at[1])
-    sq_s.start()
+    sq_s = squares_to_partner(1, sf * sf)
     ph("t_os")
-    gained = (sf * sgain[...].reshape(1, sw)).astype(bf)
     l_os.wait()
-    n_cut = c_send.shape[0]
-    cut = feats // n_cut
-    for n in range(n_cut):
-        comb[:, n * cut : (n + 1) * cut] = dot(gained, vos[:, n * cut : (n + 1) * cut])
+    copies = halves_to_partner((sf * sgain[...].reshape(1, sw)).astype(bf), vos, comb, c_send, c_recv, c_ss, c_rs)
+    ph("u_wsum")
+    sw_cols = 2.0 * sw
     sq_w.wait_recv()
-    sw_cols = 2.0 * sw
-    inv_w = lax.rsqrt((sq_send[0] + sq_recv[0])[:, :1] / sw_cols + EPS)
-    ph("u_sqwait")
-    sq_s.wait_recv()
-    ph("v_csend")
-    inv_s = lax.rsqrt((sq_send[1] + sq_recv[1])[:, :1] / sw_cols + EPS)
-    copies = []
-    theirs = pl.ds(pl.multiple_of(other * half, half), half)
-    mine = pl.ds(pl.multiple_of(t * half, half), half)
+    inv_w = lax.rsqrt((sq_send[0, mine] + sq_recv[0])[:, :1] / sw_cols + EPS)
     for n in range(n_cut):
         cols = slice(n * cut, (n + 1) * cut)
-        comb[:, cols] = comb[:, cols] * inv_s + total_w[:, cols] * inv_w
-        c_send[n] = comb[theirs, cols].astype(bf)
-        copy = to_partner(c_send.at[n], c_recv.at[n], c_ss.at[n], c_rs.at[n])
-        copy.start()
-        copies.append(copy)
+        w_copies[n].wait_recv()
+        total_w[:half, cols] = (total_w[mine, cols] + wc_recv[n].astype(f32)) * inv_w
 
     ph("w_drain")
     x_copy.wait_send()
@@ -498,23 +554,24 @@
     sq_w.wait_send()
     sq_s.wait_send()
 
+    ph("x_sqrecv")
+    sq_s.wait_recv()
+    inv_s = lax.rsqrt((sq_send[1, mine] + sq_recv[1])[:, :1] / sw_cols + EPS)
     ph("x_crecv")
     square = jnp.zeros((half, 1), f32)
     for n in range(n_cut):
         cols = slice(n * cut, (n + 1) * cut)
         copies[n].wait_recv()
-        summed = (comb[mine, cols] + c_recv[n].astype(f32)).astype(bf).astype(f32)
+        summed = (comb[mine, cols] + c_recv[n].astype(f32)) * inv_s + total_w[:half, cols]
+        summed = summed.astype(bf).astype(f32)
         total_w[:half, cols] = summed
         square = square + jnp.sum(summed * summed, axis=1, keepdims=True)
     ph("y_out")
     inv = lax.rsqrt(square / feats + EPS)
     out[...] = (total_w[:half, :] * inv * post_gain[...].reshape(1, feats)).astype(bf)
-    for copy in copies:
+    for copy in copies + w_copies:
         copy.wait_send()
     ph(None)
-
-
-SIGN = -1
 
 
 def one_kernel(n_sp, *args):
@@ -545,14 +602,15 @@
         v((3, rows, sw), f32),
         v((heads, 2, half + half // 2, wide), bf), v((n_sp, 2, half + half // 2, wide), bf),
         v((n_sp * half, wide), bf),
-        v((n_chunks, n_chunks, 4 * half, wide), f32), v((n_chunks, n_chunks, 4 * half, wide), f32),
+        v((2 * n_chunks, 2 * n_chunks, rows, wide), f32), v((2 * n_chunks, 2 * n_chunks, rows, wide), f32),
         v((rows, sw), bf), v((rows, kvw_cols), bf), v((rows, kvw_cols), bf), v((rows, sw), bf),
         v((n_sp, half // 2, wide), bf), v((heads, 2, half // 2, wide), bf), v((rows, sw), f32),
-        v((2, rows, 128), f32), v((2, rows, 128), f32), v((rows, feats), f32), v((rows, feats), f32),
+        v((2, rows, 128), f32), v((2, half, 128), f32), v((rows, feats), f32), v((rows, feats), f32),
+        v((n_cut, half, feats // n_cut), bf), v((n_cut, half, feats // n_cut), bf),
         v((n_cut, half, feats // n_cut), bf), v((n_cut, half, feats // n_cut), bf),
         dma((14,)), dma((6,)), dma, dma, dma, dma, dma, dma((heads, 2)), dma((n_sp,)),
         dma((n_sp,)), dma((n_sp,)), dma, dma, dma((n_sp,)), dma((heads, 2)), dma((2,)), dma((2,)),
-        dma((n_cut,)), dma((n_cut,)),
+        dma((n_cut,)), dma((n_cut,)), dma((n_cut,)), dma((n_cut,)), pltpu.SemaphoreType.REGULAR, pltpu.SemaphoreType.REGULAR,
     ]
     return pl.pallas_call(
         functools.partial(kernel, n_sp),

time: 33.8 us -> 30.5 us (0.902)
  Pallas kernels: 33 us -> 29.6 us
    pallas_call x1, Pallas kernels: 33 us -> 29.6 us  [one_kernel(): pl.pallas_call(functools.partial(kernel, n_sp), out_shape=pltpu.VMEM((hal...]
where the time goes in v2:
time: 30.5 us; the launch traced here: 30.3 us
  Pallas kernels  29.6 us (97%)
  local copies, waits for them, and re-layouts  0.71 us (2%)
    pallas_call x1, Pallas kernels, one_kernel(): pl.pallas_call(functools.partial(kernel, n_sp), out_shape=pltpu.VMEM((hal...  29.6 us
    unnamed x1, local copies, waits for them, and re-layouts  0.71 us

profile of v2, /device:TPU:0, one launch (start us, length us, event | category | flops | bytes accessed | tf_op | source)
XLA Modules:
  0.0 30.3 jit_solution(10153044449041077499)
XLA Ops:
  0.0 29.6 %layer.1 = bf16[64,2048]{1,0:T(8,128)(2,1)S(1)} custom-call(bf16[128,1024]{1,0:T(8,128)(2,1)} %tokens.1, f32[2048]{0:T(1024)} %pre_gain_in.1, bf16[2048,512]{1,0:T(8,128)(2,1)} %wqs.1, bf16[2048,512]{1,0:T(8,128)(2,1)} %wks.1, bf16[2048,512]{1,0:T(8,128)(2,1)} %wvs.1, bf16[2048,512]{1,0:T(8,128)(2,1)} %wqw.1, bf16[2048,256]{1,0:T(8,128)(2,1)} %wkw.1, ...), custom_call_target="tpu_custom_call" | custom-call | tf_op jit(solution)/shard_map/layer/pallas_call | solution.py:615
  29.6 0.7 %copy.17 = bf16[64,2048]{1,0:T(8,128)(2,1)} copy(bf16[64,2048]{1,0:T(8,128)(2,1)S(1)} %layer.1) | data formatting | bytes 524288

commit v3 on v2

--- a/solution.py
+++ b/solution.py
@@ -49,7 +49,17 @@
 
 
 def send_order(z, count):
-    return sorted(range(count), key=lambda c: (abs(c - z), 2 * c // count != 2 * z // count))
+    near = [c for c in zone_order(z, count) if 2 * c // count == 2 * z // count]
+    far = [c for c in reversed(range(count)) if c not in near]
+    if z >= count // 2:
+        far.reverse()
+    inside = [(c, y) for c in near for y in range(2)]
+    across = [(c, (y + n) % 2) for y in range(2) for n, c in enumerate(far)]
+    return inside + across if IN_FIRST else across + inside
+
+
+IN_FIRST = False
+AHEAD = 4
 
 
 def kernel(
@@ -57,7 +67,7 @@
     tokens, pre_gain_in, wqs, wks, wvs, wqw, wkw, wvw, bias_in, sinks_in, sgain_in, wgain_in, wos, wow,
     post_gain_in, out,
     pre_gain, bias, sinks, sgain, wgain, post_gain, x, bias_buf, xg, vqs, vks, vvs, vqw, vkw, vvw, vos, vow,
-    proj, kv_send, kv_all, q_pad, part, mass,
+    proj, kv_send, kv_all, q_pad, acc, mass,
     qw, kvw, kvw_prev, w_out_buf, o_send, o_recv, s_out_buf,
     sq_send, sq_recv, total_w, comb, c_send, c_recv, wc_send, wc_recv,
     w_sem, small_sem, tok_sem, x_ss, x_rs, b_ss, b_rs, kv_ss, kv_rs, f_ss, f_rs,
@@ -216,7 +226,7 @@
     def dest_order(n):
         by_zone = []
         for z in range(n_chunks):
-            order = [2 * c + y for c in send_order(z, n_chunks) for y in range(2)]
+            order = [2 * c + y for c, y in send_order(z, n_chunks)]
             by_zone.append(order[n])
         return chosen(zone, by_zone)
 
@@ -322,32 +332,26 @@
     def queries_of(g, count):
         return q_pad[pl.ds(pl.multiple_of(g * rows, rows), count * rows), :]
 
-    def take_zone(c, others):
-        places = [(2 * c + 1, 2 * c + 1, 1, True), (2 * c, 2 * c, 2, True)]
-        for e in others:
-            qc, kc = jnp.maximum(c, e), jnp.minimum(c, e)
-            places += [(2 * qc, 2 * kc, 2, False), (2 * qc, 2 * kc + 1, 2, False)]
-        step = 4
-        for n in range(0, len(places), step):
-            some = places[n : n + step]
-            results = weigh([(queries_of(q, count), keys_of(g), masked) for q, g, count, masked in some])
-            for (q, g, count, _), (res, total) in zip(some, results):
-                part[g, pl.ds(q, count)] = res.reshape(count, rows, 2 * hd)
-                mass[g, pl.ds(q, count)] = total.reshape(count, rows, 2 * hd)
-
-    def finish(g):
-        def add(j, carry):
-            acc, passed = carry
-            k = g - j
-            return acc + jnp.exp2(-passed) * part[k, g], passed + mass[k, g]
-
-        acc, _ = lax.fori_loop(1, g + 1, add, (part[g, g], mass[g, g]))
-        for b in range(2):
-            top = acc[b * half : b * half + quarter, hd:]
-            bot = acc[b * half + quarter : (b + 1) * half, hd:]
-            o_send[2 * g + b] = jnp.concatenate([top, bot], axis=1).astype(bf)
-        for b in range(2):
-            k = 2 * g + b
+    def put(q, g, count, result, first):
+        res, total = (value.reshape(count, rows, 2 * hd) for value in result)
+        at = pl.ds(q, count)
+        if first:
+            acc[at] = res
+            mass[at] = total
+        else:
+            passed = mass[at]
+            acc[at] = acc[at] + jnp.exp2(-passed) * res
+            mass[at] = passed + total
+
+    def give(c):
+        for g in range(2):
+            value = acc[2 * c + g]
+            for b in range(2):
+                top = value[b * half : b * half + quarter, hd:]
+                bot = value[b * half + quarter : (b + 1) * half, hd:]
+                o_send[4 * c + 2 * g + b] = jnp.concatenate([top, bot], axis=1).astype(bf)
+        for b in range(4):
+            k = 4 * c + b
             is_self = jnp.logical_and(k == s, t == owner)
 
             @pl.when(is_self)
@@ -361,57 +365,74 @@
                     recv_sem=o_rs.at[slot, t], device_id={"sp": k, "tp": owner}, device_id_type=MESH,
                 ).start()
 
-    def finish_range(lo, hi):
-        def step(g, carry):
-            finish(g)
-            return carry
-
-        lax.fori_loop(lo, hi, step, 0)
-
     takes = [zone_order(z, n_chunks) for z in range(n_chunks)]
-    units = []
-    for z in range(n_chunks):
-        mine_units = [[2 * c, 2 * c + 1] for c in takes[z]]
-        units.append(mine_units)
-    n_units = len(units[0])
-    ends = []
-    for z in range(n_chunks):
-        seen, done, spans = set(), 0, []
-        for unit in units[z]:
-            seen |= set(unit)
-            upto = done
-            while upto in seen:
-                upto += 1
-            spans.append((done, upto))
-            done = upto
-        ends.append(spans)
-    group = [[chosen(zone, [units[z][n][m] for z in range(n_chunks)]) for m in range(len(units[0][n]))] for n in range(n_units)]
+    batches = []
+    for n in range(n_chunks):
+        partners = [sorted(takes[z][:n], reverse=True) for z in range(n_chunks)]
+        steps = [[None] + list(range(min(n, 1)))] + [list(range(m, min(m + 2, n))) for m in range(1, n, 2)]
+        batches.append((partners, steps))
+    seen = [set() for _ in range(n_chunks)]
+    given = [set() for _ in range(n_chunks)]
 
     def arrive(n):
-        for g in group[n]:
-            for b in range(2):
-                forward(2 * g + b)
-        for g in group[n]:
-            for b in range(2):
-                take_q(2 * g + b)
-
-    def arrived(n):
-        for g in group[n]:
-            for b in range(2):
-                forward_arrived(2 * g + b)
+        c = chosen(zone, [takes[z][n] for z in range(n_chunks)])
+        for b in range(4):
+            forward(4 * c + b)
+        for b in range(4):
+            take_q(4 * c + b)
+
+    def take(n):
+        c = chosen(zone, [takes[z][n] for z in range(n_chunks)])
+        for b in range(4):
+            forward_arrived(4 * c + b)
+        partners, steps = batches[n]
+        for step in steps:
+            places = []
+            for m in step:
+                if m is None:
+                    places += [(2 * c + 1, 2 * c + 1, 1, True), (2 * c, 2 * c, 2, True)]
+                else:
+                    e = chosen(zone, [partners[z][m] for z in range(n_chunks)])
+                    qc, kc = jnp.maximum(c, e), jnp.minimum(c, e)
+                    places += [(2 * qc, 2 * kc + 1, 2, False), (2 * qc, 2 * kc, 2, False)]
+            results = weigh([(queries_of(q, count), keys_of(g), masked) for q, g, count, masked in places])
+            if step[0] is None:
+                (res1, total1), (res0, total0) = results[:2]
+                at = pl.ds(2 * c, 2)
+                acc[at] = jnp.concatenate(
+                    [res0[:rows], res1 + jnp.exp2(-total1) * res0[rows:]], axis=0
+                ).reshape(2, rows, 2 * hd)
+                mass[at] = jnp.concatenate([total0[:rows], total1 + total0[rows:]], axis=0).reshape(2, rows, 2 * hd)
+            for (q, g, count, masked), result in zip(places, results):
+                if not masked:
+                    put(q, g, count, result, False)
+            ready = []
+            for z in range(n_chunks):
+                for m in step:
+                    a, b = takes[z][n], takes[z][n] if m is None else partners[z][m]
+                    seen[z].add((max(a, b), min(a, b)))
+                ready.append([
+                    q for q in range(n_chunks)
+                    if q not in given[z] and all((q, k) in seen[z] for k in range(q + 1))
+                ])
+                given[z] |= set(ready[z])
+            for j in range(max(len(r) for r in ready)):
+                lasts = chosen(zone, [r[j] if j < len(r) else 0 for r in ready])
+                if all(j < len(r) for r in ready):
+                    give(lasts)
+                else:
+                    @pl.when(chosen(zone, [int(j < len(r)) for r in ready]) == 1)
+                    def _():
+                        give(lasts)
 
     ph("l_arrive0")
     arrive(0)
-    for n in range(n_units):
-        if n + 1 < n_units:
+    for n in range(n_chunks):
+        if n + 1 < n_chunks:
             ph(f"m{n}_arrive")
             arrive(n + 1)
-        ph(f"m{n}_fwdarr")
-        arrived(n)
-        ph(f"m{n}_tiles")
-        take_zone(group[n][0] // 2, [group[m][0] // 2 for m in range(n)])
-        ph(f"m{n}_finish")
-        finish_range(chosen(zone, [ends[z][n][0] for z in range(n_chunks)]), chosen(zone, [ends[z][n][1] for z in range(n_chunks)]))
+        ph(f"m{n}_take")
+        take(n)
 
     ph("n_prev")
 
@@ -462,13 +483,20 @@
 
     def halves_to_partner(left, weights, total, send, recv, ss, rs):
         copies = []
+
+        def give_half(n):
+            send[n] = total[theirs, n * cut : (n + 1) * cut].astype(bf)
+            copy = to_partner(send.at[n], recv.at[n], ss.at[n], rs.at[n])
+            copy.start()
+            copies.append(copy)
+
         for n in range(n_cut):
             cols = slice(n * cut, (n + 1) * cut)
             total[:, cols] = dot(left, weights[:, cols])
-            send[n] = total[theirs, cols].astype(bf)
-            copy = to_partner(send.at[n], recv.at[n], ss.at[n], rs.at[n])
-            copy.start()
-            copies.append(copy)
+            if n >= AHEAD:
+                give_half(n - AHEAD)
+        for n in range(n_cut - AHEAD, n_cut):
+            give_half(n)
         return copies
 
     wf = w_out_buf[...].astype(f32)
@@ -528,13 +556,13 @@
 
         return carry
 
-    lax.fori_loop(0, 2 * heads, scatter_done, 0)
+    lax.fori_loop(0, 2 * heads, scatter_done, 0, unroll=True)
 
     def forward_sent(k, carry):
         to_partner(kv_all.at[k, t, :half], kv_all.at[k, t, :half], f_ss.at[k], f_rs.at[k]).wait_send()
         return carry
 
-    lax.fori_loop(0, n_sp, forward_sent, 0)
+    lax.fori_loop(0, n_sp, forward_sent, 0, unroll=True)
 
     @pl.when(s < n_sp - 1)
     def _():
@@ -550,7 +578,7 @@
 
         return carry
 
-    lax.fori_loop(0, n_sp, gave, 0)
+    lax.fori_loop(0, n_sp, gave, 0, unroll=True)
     sq_w.wait_send()
     sq_s.wait_send()
 
@@ -602,7 +630,7 @@
         v((3, rows, sw), f32),
         v((heads, 2, half + half // 2, wide), bf), v((n_sp, 2, half + half // 2, wide), bf),
         v((n_sp * half, wide), bf),
-        v((2 * n_chunks, 2 * n_chunks, rows, wide), f32), v((2 * n_chunks, 2 * n_chunks, rows, wide), f32),
+        v((2 * n_chunks, rows, wide), f32), v((2 * n_chunks, rows, wide), f32),
         v((rows, sw), bf), v((rows, kvw_cols), bf), v((rows, kvw_cols), bf), v((rows, sw), bf),
         v((n_sp, half // 2, wide), bf), v((heads, 2, half // 2, wide), bf), v((rows, sw), f32),
         v((2, rows, 128), f32), v((2, half, 128), f32), v((rows, feats), f32), v((rows, feats), f32),

time: 30.5 us -> 29.2 us (0.957)
  Pallas kernels: 29.6 us -> 28.2 us
    pallas_call x1, Pallas kernels: 29.6 us -> 28.2 us  [one_kernel(): pl.pallas_call(functools.partial(kernel, n_sp), out_shape=pltpu.VMEM((hal...]
where the time goes in v3:
time: 29.2 us; the launch traced here: 28.9 us
  Pallas kernels  28.2 us (97%)
  local copies, waits for them, and re-layouts  0.71 us (2%)
    pallas_call x1, Pallas kernels, one_kernel(): pl.pallas_call(functools.partial(kernel, n_sp), out_shape=pltpu.VMEM((hal...  28.2 us
    unnamed x1, local copies, waits for them, and re-layouts  0.71 us

profile of v3, /device:TPU:0, one launch (start us, length us, event | category | flops | bytes accessed | tf_op | source)
XLA Modules:
  0.0 28.9 jit_solution(11839826347716729987)
XLA Ops:
  0.0 28.2 %layer.1 = bf16[64,2048]{1,0:T(8,128)(2,1)S(1)} custom-call(bf16[128,1024]{1,0:T(8,128)(2,1)} %tokens.1, f32[2048]{0:T(1024)} %pre_gain_in.1, bf16[2048,512]{1,0:T(8,128)(2,1)} %wqs.1, bf16[2048,512]{1,0:T(8,128)(2,1)} %wks.1, bf16[2048,512]{1,0:T(8,128)(2,1)} %wvs.1, bf16[2048,512]{1,0:T(8,128)(2,1)} %wqw.1, bf16[2048,256]{1,0:T(8,128)(2,1)} %wkw.1, ...), custom_call_target="tpu_custom_call" | custom-call | tf_op jit(solution)/shard_map/layer/pallas_call | solution.py:643
  28.2 0.7 %copy.17 = bf16[64,2048]{1,0:T(8,128)(2,1)} copy(bf16[64,2048]{1,0:T(8,128)(2,1)S(1)} %layer.1) | data formatting | bytes 524288

commit v4 on v2

--- a/solution.py
+++ b/solution.py
@@ -36,32 +36,25 @@
     return lax.dot_general(a, b, (((1,), (1,)), ((), ())), preferred_element_type=jnp.float32)
 
 
-def chosen(at, table):
-    value = jnp.int32(table[0])
-    for n in range(1, len(table)):
-        if table[n] != table[0]:
-            value = jnp.where(at == n, jnp.int32(table[n]), value)
-    return value
-
-
-def zone_order(z, count):
-    return sorted(range(count), key=lambda c: (2 * c // count != 2 * z // count, abs(c - z)))
-
-
-def send_order(z, count):
-    return sorted(range(count), key=lambda c: (abs(c - z), 2 * c // count != 2 * z // count))
+TILE_BLOCKS = 2
+AHEAD = 4
+OWN_LAST = 1
+PREV_AT = 1
+UP_AT = 0
+DOWN_AT = 0
+HLB_FIRST = False
 
 
 def kernel(
     n_sp,
     tokens, pre_gain_in, wqs, wks, wvs, wqw, wkw, wvw, bias_in, sinks_in, sgain_in, wgain_in, wos, wow,
     post_gain_in, out,
-    pre_gain, bias, sinks, sgain, wgain, post_gain, x, bias_buf, xg, vqs, vks, vvs, vqw, vkw, vvw, vos, vow,
-    proj, kv_send, kv_all, q_pad, part, mass,
-    qw, kvw, kvw_prev, w_out_buf, o_send, o_recv, s_out_buf,
+    pre_gain, bias, sinks, sgain, wgain, post_gain, x, xg, vqs, vks, vvs, vqw, vkw, vvw, vos, vow,
+    proj, kv_send, kv_all, q_pad, acc, mass,
+    qw, kvw, kvw_prev, w_out_buf, o_send, o_recv, late_send, late_recv, s_out_buf,
     sq_send, sq_recv, total_w, comb, c_send, c_recv, wc_send, wc_recv,
-    w_sem, small_sem, tok_sem, x_ss, x_rs, b_ss, b_rs, kv_ss, kv_rs, f_ss, f_rs,
-    p_ss, p_rs, o_ss, o_rs, sq_ss, sq_rs, c_ss, c_rs, wc_ss, wc_rs, hello, all_in,
+    w_sem, small_sem, tok_sem, x_ss, x_rs, kv_ss, kv_rs, far_ss,
+    p_ss, p_rs, o_ss, o_rs, late_ss, late_rs, sq_ss, sq_rs, c_ss, c_rs, wc_ss, wc_rs, hello, all_in,
 ):
     bf = jnp.bfloat16
     f32 = jnp.float32
@@ -71,12 +64,11 @@
     rows, feat_half = tokens.shape
     feats = 2 * feat_half
     half = rows // 2
-    quarter = half // 2
     hd = HEAD_DIM
     heads = wqs.shape[1] // hd
     kv_heads = wkw.shape[1] // hd
     sw = wqs.shape[1]
-    n_chunks = n_sp // 4
+    blocks_in_zone = heads // 2
     ph = Phases()
     ph("a_entry")
 
@@ -147,12 +139,6 @@
     for load in smalls:
         load.wait()
 
-    row_id = lax.broadcasted_iota(jnp.int32, (heads, 128), 0)
-    bias_rows = jnp.zeros((heads, 128), f32)
-    for i in range(heads):
-        bias_rows = jnp.where(row_id == i, bias[i] * LOG2E, bias_rows)
-    bias_buf[t] = bias_rows
-
     ph("c_gain")
     gain = pre_gain[...].reshape(1, feats)
     gains = [
@@ -166,9 +152,6 @@
         return jnp.sum(value * value, axis=1, keepdims=True)
 
     squares = scaled(0)
-
-    b_copy = to_partner(bias_buf.at[t], bias_buf.at[t], b_ss, b_rs)
-    b_copy.start()
 
     ph("e_own")
     for n, (name, w) in enumerate([("ks", vks), ("vs", vvs), ("qs", vqs)]):
@@ -187,15 +170,11 @@
     values = (proj[1] + dot(xg[1], vvs[1])) * inv
     for i in range(heads):
         cols = slice(i * hd, (i + 1) * hd)
-        packed = jnp.concatenate([keys[:, cols], values[:, cols]], axis=1).astype(bf)
-        kv_send[i, :, :half] = packed.reshape(2, half, 2 * hd)
+        kv_send[i, :rows] = jnp.concatenate([keys[:, cols], values[:, cols]], axis=1).astype(bf)
     queries = (proj[2] + dot(xg[1], vqs[1])) * (inv * (LOG2E * hd**-0.5))
     for i in range(heads):
         cols = slice(i * hd, (i + 1) * hd)
-        for u in range(2):
-            top = queries[u * half : u * half + quarter, cols]
-            low = queries[u * half + quarter : (u + 1) * half, cols]
-            kv_send[i, u, half:] = jnp.concatenate([top, low], axis=1).astype(bf)
+        kv_send[i, rows:] = jnp.concatenate([queries[:half, cols], queries[half:, cols]], axis=1).astype(bf)
 
     ph("h_barrier")
 
@@ -209,33 +188,59 @@
         pl.semaphore_wait(all_in, 1)
 
     ph("i_scatter")
-    zone = s // 4
-    owner = lax.rem(s, 2)
-    slot = s // 2
-
-    def dest_order(n):
-        by_zone = []
-        for z in range(n_chunks):
-            order = [2 * c + y for c in send_order(z, n_chunks) for y in range(2)]
-            by_zone.append(order[n])
-        return chosen(zone, by_zone)
+    side = s // heads
+    slot = lax.rem(s, heads)
+    plane = lax.rem(s // blocks_in_zone, 2)
+    first = side * heads
+    above = lax.rem(slot + t, 2) == 0
+    below = jnp.logical_not(above)
+    lower = side == 0
+    upper = side == 1
+
+    across = [n // 2 + (n % 2) * (heads // 4) for n in range(heads // 2)]
+
+    def far_copy(m, part_of):
+        i = 2 * m + lax.rem(t + side, 2)
+        return pltpu.make_async_remote_copy(
+            src_ref=kv_send.at[i, part_of], dst_ref=kv_all.at[s, part_of], send_sem=far_ss.at[m],
+            recv_sem=kv_rs.at[s], device_id={"sp": (1 - side) * heads + i, "tp": t}, device_id_type=MESH,
+        )
+
+    keys_part, queries_part = slice(0, rows), slice(rows, rows + half)
+
+    def near_copy(i):
+        return pltpu.make_async_remote_copy(
+            src_ref=kv_send.at[i], dst_ref=kv_all.at[s], send_sem=kv_ss.at[i],
+            recv_sem=kv_rs.at[s], device_id={"sp": first + i, "tp": t}, device_id_type=MESH,
+        )
+
+    def send_far(moment):
+        if moment == UP_AT:
+            @pl.when(lower)
+            def _():
+                for m in across:
+                    far_copy(m, keys_part).start()
+
+        if moment == DOWN_AT:
+            @pl.when(upper)
+            def _():
+                for m in across:
+                    far_copy(m, queries_part).start()
+
+    def send_near(n):
+        i = lax.rem(n + (OWN_LAST - plane) * (OWN_LAST * 2 - 1) * (heads // 2), heads)
+
+        @pl.when(i == slot)
+        def _():
+            pltpu.make_async_copy(kv_send.at[i], kv_all.at[s], kv_rs.at[s]).start()
+
+        @pl.when(i != slot)
+        def _():
+            near_copy(i).start()
 
     for n in range(heads):
-        i = dest_order(n)
-        chip = 2 * i + t
-        for u in range(2):
-            is_self = jnp.logical_and(chip == s, u == t)
-
-            @pl.when(is_self)
-            def _():
-                pltpu.make_async_copy(kv_send.at[i, u], kv_all.at[s, u], kv_rs.at[s]).start()
-
-            @pl.when(jnp.logical_not(is_self))
-            def _():
-                pltpu.make_async_remote_copy(
-                    src_ref=kv_send.at[i, u], dst_ref=kv_all.at[s, u], send_sem=kv_ss.at[i, u],
-                    recv_sem=kv_rs.at[s], device_id={"sp": chip, "tp": u}, device_id_type=MESH,
-                ).start()
+        send_near(n)
+    send_far(0)
 
     ph("j_wproj")
     l_ow.start()
@@ -249,48 +254,39 @@
         device_id={"sp": to, "tp": t}, device_id_type=MESH,
     )
 
-    @pl.when(s < n_sp - 1)
-    def _():
-        prev_copy(s + 1).start()
-
     for load in loads["qw"]:
         load.wait()
     qw[...] = ((dot(xg[0], vqw[0]) + dot(xg[1], vqw[1])) * inv).astype(bf)
 
+    send_far(1)
+
+    def send_prev():
+        @pl.when(s < n_sp - 1)
+        def _():
+            prev_copy(s + 1).start()
+
     ph("k_misc")
-
-    def forward(src):
-        pltpu.make_async_remote_copy(
-            src_ref=kv_send.at[0, 0], dst_ref=kv_all.at[src, t], send_sem=kv_ss.at[0, 0],
-            recv_sem=kv_rs.at[src], device_id={"sp": s, "tp": other}, device_id_type=MESH,
-        ).wait_recv()
-        to_partner(kv_all.at[src, t, :half], kv_all.at[src, t, :half], f_ss.at[src], f_rs.at[src]).start()
-
-    def forward_arrived(k):
-        to_partner(kv_all.at[k, other, :half], kv_all.at[k, other, :half], f_ss.at[k], f_rs.at[k]).wait_recv()
-
-    def take_q(k):
-        slab = kv_all[k, t, half:].astype(f32)
-        zero = jnp.zeros((quarter, hd), f32)
-        both = jnp.concatenate(
-            [
-                jnp.concatenate([slab[:, :hd], zero], axis=1),
-                jnp.concatenate([slab[:, hd:], zero], axis=1),
-            ],
-            axis=0,
-        )
-        q_pad[pl.ds(pl.multiple_of(k * half, half), half), :] = both.astype(bf)
-
-    b_copy.wait_recv()
-    head_bias = bias_buf[owner, pl.ds(slot, 1), :][:, :1]
-
-    kt = 2 * rows
+    head_bias = bias[slot] * LOG2E
+    kt = TILE_BLOCKS * rows
+    zone = blocks_in_zone * rows
     later = (
         lax.broadcasted_iota(jnp.int32, (kt, kt), 0) > lax.broadcasted_iota(jnp.int32, (kt, kt), 1)
     ).astype(bf)
-    row = lax.broadcasted_iota(jnp.int32, (rows, kt), 0)
-    lane = lax.broadcasted_iota(jnp.int32, (rows, kt), 1)
-    before = lane < (row // half) * rows + t * half + lax.rem(row, half)
+    before = lax.broadcasted_iota(jnp.int32, (kt, kt), 1) < lax.broadcasted_iota(jnp.int32, (kt, kt), 0)
+
+    def landed(src, ref):
+        pltpu.make_async_remote_copy(
+            src_ref=ref, dst_ref=ref, send_sem=kv_ss.at[0], recv_sem=kv_rs.at[src],
+            device_id=partner, device_id_type=MESH,
+        ).wait_recv()
+
+    def take_q(k):
+        slab = kv_all[k, rows:].astype(f32)
+        zero = jnp.zeros((half, hd), f32)
+        both = jnp.concatenate(
+            [jnp.concatenate([slab[:, :hd], zero], axis=1), jnp.concatenate([slab[:, hd:], zero], axis=1)], axis=0
+        )
+        q_pad[pl.ds(pl.multiple_of(k * rows, rows), rows), :] = both.astype(bf)
 
     def weigh(tiles):
         drops, holds = [], []
@@ -300,13 +296,13 @@
             drop = pos + jnp.log2(1.0 + jnp.exp2(z - pos - pos))
             hold = z - drop
             if masked:
-                drop_top = jnp.where(before, drop[:rows], 0.0)
-                hold_top = jnp.where(before, hold[:rows], -jnp.inf)
-                if drop.shape[0] == rows:
+                drop_top = jnp.where(before, drop[:kt], 0.0)
+                hold_top = jnp.where(before, hold[:kt], -jnp.inf)
+                if drop.shape[0] == kt:
                     drop, hold = drop_top, hold_top
                 else:
-                    drop = jnp.concatenate([drop_top, drop[rows:]], axis=0)
-                    hold = jnp.concatenate([hold_top, hold[rows:]], axis=0)
+                    drop = jnp.concatenate([drop_top, drop[kt:]], axis=0)
+                    hold = jnp.concatenate([hold_top, hold[kt:]], axis=0)
             drops.append(drop)
             holds.append(hold)
         suffixes = [dot(drop.astype(bf), later) for drop in drops]
@@ -316,102 +312,141 @@
             results.append((dot(jnp.exp2(hold - suffix).astype(bf), kv), total))
         return results
 
-    def keys_of(g):
-        return kv_all[pl.ds(2 * g, 2), :, :half].reshape(kt, 2 * hd)
-
-    def queries_of(g, count):
-        return q_pad[pl.ds(pl.multiple_of(g * rows, rows), count * rows), :]
-
-    def take_zone(c, others):
-        places = [(2 * c + 1, 2 * c + 1, 1, True), (2 * c, 2 * c, 2, True)]
-        for e in others:
-            qc, kc = jnp.maximum(c, e), jnp.minimum(c, e)
-            places += [(2 * qc, 2 * kc, 2, False), (2 * qc, 2 * kc + 1, 2, False)]
-        step = 4
-        for n in range(0, len(places), step):
-            some = places[n : n + step]
-            results = weigh([(queries_of(q, count), keys_of(g), masked) for q, g, count, masked in some])
-            for (q, g, count, _), (res, total) in zip(some, results):
-                part[g, pl.ds(q, count)] = res.reshape(count, rows, 2 * hd)
-                mass[g, pl.ds(q, count)] = total.reshape(count, rows, 2 * hd)
-
-    def finish(g):
-        def add(j, carry):
-            acc, passed = carry
-            k = g - j
-            return acc + jnp.exp2(-passed) * part[k, g], passed + mass[k, g]
-
-        acc, _ = lax.fori_loop(1, g + 1, add, (part[g, g], mass[g, g]))
-        for b in range(2):
-            top = acc[b * half : b * half + quarter, hd:]
-            bot = acc[b * half + quarter : (b + 1) * half, hd:]
-            o_send[2 * g + b] = jnp.concatenate([top, bot], axis=1).astype(bf)
-        for b in range(2):
-            k = 2 * g + b
-            is_self = jnp.logical_and(k == s, t == owner)
-
-            @pl.when(is_self)
+    def keys_of(c, n):
+        return kv_all[pl.ds(blocks_in_zone * c + TILE_BLOCKS * n, TILE_BLOCKS), :rows].reshape(kt, 2 * hd)
+
+    def rows_of(c, count):
+        return pl.ds(pl.multiple_of(c * zone, zone), count)
+
+    def add(at, result):
+        passed = mass[at]
+        acc[at] = acc[at] + jnp.exp2(-passed) * result[0]
+        mass[at] = passed + result[1]
+
+    def own_pairs(c):
+        at = rows_of(c, zone)
+        qs = q_pad[at]
+        (res1, total1), (res0, total0) = weigh([(qs[kt:], keys_of(c, 1), True), (qs, keys_of(c, 0), True)])
+        acc[at] = jnp.concatenate([res0[:kt], res1 + jnp.exp2(-total1) * res0[kt:]], axis=0)
+        mass[at] = jnp.concatenate([total0[:kt], total1 + total0[kt:]], axis=0)
+
+    def cross_pairs(qc, kc, fresh):
+        at = rows_of(qc, zone)
+        qs = q_pad[at]
+        one, two_ = weigh([(qs, keys_of(kc, 1), False), (qs, keys_of(kc, 0), False)])
+        if fresh:
+            acc[at] = one[0] + jnp.exp2(-one[1]) * two_[0]
+            mass[at] = one[1] + two_[1]
+        else:
+            add(at, one)
+            add(at, two_)
+
+    def o_copy(k):
+        return pltpu.make_async_remote_copy(
+            src_ref=o_send.at[k], dst_ref=o_recv.at[slot], send_sem=o_ss.at[k], recv_sem=o_rs.at[slot],
+            device_id={"sp": k, "tp": t}, device_id_type=MESH,
+        )
+
+    def give(zones):
+        blocks = [blocks_in_zone * c + b for c in zones for b in range(blocks_in_zone)]
+        for k in blocks:
+            value = acc[pl.ds(pl.multiple_of(k * rows, rows), rows), :][:, hd:]
+            o_send[k] = jnp.concatenate([value[:half], value[half:]], axis=1).astype(bf)
+        for k in blocks:
+
+            @pl.when(k == s)
             def _():
-                pltpu.make_async_copy(o_send.at[k], o_recv.at[slot, t], o_rs.at[slot, t]).start()
-
-            @pl.when(jnp.logical_not(is_self))
+                pltpu.make_async_copy(o_send.at[k], o_recv.at[slot], o_rs.at[slot]).start()
+
+            @pl.when(k != s)
             def _():
-                pltpu.make_async_remote_copy(
-                    src_ref=o_send.at[k], dst_ref=o_recv.at[slot, t], send_sem=o_ss.at[k],
-                    recv_sem=o_rs.at[slot, t], device_id={"sp": k, "tp": owner}, device_id_type=MESH,
-                ).start()
-
-    def finish_range(lo, hi):
-        def step(g, carry):
-            finish(g)
-            return carry
-
-        lax.fori_loop(lo, hi, step, 0)
-
-    takes = [zone_order(z, n_chunks) for z in range(n_chunks)]
-    units = []
-    for z in range(n_chunks):
-        mine_units = [[2 * c, 2 * c + 1] for c in takes[z]]
-        units.append(mine_units)
-    n_units = len(units[0])
-    ends = []
-    for z in range(n_chunks):
-        seen, done, spans = set(), 0, []
-        for unit in units[z]:
-            seen |= set(unit)
-            upto = done
-            while upto in seen:
-                upto += 1
-            spans.append((done, upto))
-            done = upto
-        ends.append(spans)
-    group = [[chosen(zone, [units[z][n][m] for z in range(n_chunks)]) for m in range(len(units[0][n]))] for n in range(n_units)]
-
-    def arrive(n):
-        for g in group[n]:
-            for b in range(2):
-                forward(2 * g + b)
-        for g in group[n]:
-            for b in range(2):
-                take_q(2 * g + b)
-
-    def arrived(n):
-        for g in group[n]:
-            for b in range(2):
-                forward_arrived(2 * g + b)
+                o_copy(k).start()
+
+    def late_copy(j):
+        return pltpu.make_async_remote_copy(
+            src_ref=late_send.at[j], dst_ref=late_recv.at[slot // 2], send_sem=late_ss.at[j],
+            recv_sem=late_rs.at[slot // 2], device_id={"sp": first + j, "tp": t}, device_id_type=MESH,
+        )
+
+    def give_late():
+        low_lanes = lax.broadcasted_iota(jnp.int32, (rows, 2 * hd), 1) < hd
+        for j in range(heads):
+            at = pl.ds(pl.multiple_of((first + j) * rows, rows), rows)
+            value = jnp.where(low_lanes, jnp.exp2(-mass[at]), acc[at])
+            swapped = jnp.concatenate([value[:, hd:], value[:, :hd]], axis=1)
+            late_send[j] = jnp.where(lax.rem(slot, 2) == 1, value, swapped).astype(bf)
+        for j in range(heads):
+
+            @pl.when(j == slot)
+            def _():
+                pltpu.make_async_copy(late_send.at[j], late_recv.at[slot // 2], late_rs.at[slot // 2]).start()
+
+            @pl.when(j != slot)
+            def _():
+                late_copy(j).start()
+
+    own_zone = 2 * side + plane
+    next_zone = 2 * side + 1 - plane
+
+    def arrive(c):
+        for b in range(blocks_in_zone):
+            landed(blocks_in_zone * c + b, kv_all.at[blocks_in_zone * c + b])
+        for b in range(blocks_in_zone):
+            take_q(blocks_in_zone * c + b)
 
     ph("l_arrive0")
-    arrive(0)
-    for n in range(n_units):
-        if n + 1 < n_units:
-            ph(f"m{n}_arrive")
-            arrive(n + 1)
-        ph(f"m{n}_fwdarr")
-        arrived(n)
-        ph(f"m{n}_tiles")
-        take_zone(group[n][0] // 2, [group[m][0] // 2 for m in range(n)])
-        ph(f"m{n}_finish")
-        finish_range(chosen(zone, [ends[z][n][0] for z in range(n_chunks)]), chosen(zone, [ends[z][n][1] for z in range(n_chunks)]))
+    arrive(own_zone)
+    send_far(2)
+    if PREV_AT == 0:
+        send_prev()
+    ph("l_own0")
+    own_pairs(own_zone)
+    ph("m_arrive1")
+    arrive(next_zone)
+    send_far(3)
+    if PREV_AT == 1:
+        send_prev()
+    def lower_pairs():
+        @pl.when(jnp.logical_and(lower, below))
+        def _():
+            for c in (2, 3):
+                for b in range(blocks_in_zone):
+                    landed(blocks_in_zone * c + b, kv_all.at[blocks_in_zone * c + b, rows:])
+                for b in range(blocks_in_zone):
+                    take_q(blocks_in_zone * c + b)
+                cross_pairs(c, 1, True)
+                cross_pairs(c, 0, False)
+                give([c])
+
+    ph("m_hlb")
+    if HLB_FIRST:
+        lower_pairs()
+    ph("m_own1")
+    own_pairs(next_zone)
+    cross_pairs(2 * side + 1, 2 * side, False)
+    ph("m_give")
+
+    @pl.when(lower)
+    def _():
+        give(range(2))
+
+    @pl.when(jnp.logical_and(upper, below))
+    def _():
+        give_late()
+
+    ph("m_hla")
+    if not HLB_FIRST:
+        lower_pairs()
+
+    @pl.when(jnp.logical_and(upper, above))
+    def _():
+        at = rows_of(2, 2 * zone)
+        for c in (1, 0):
+            for b in range(blocks_in_zone):
+                landed(blocks_in_zone * c + b, kv_all.at[blocks_in_zone * c + b, :rows])
+            for n in (1, 0):
+                add(at, weigh([(q_pad[at], keys_of(c, n), False)])[0])
+        give((2, 3))
 
     ph("n_prev")
 
@@ -462,13 +497,20 @@
 
     def halves_to_partner(left, weights, total, send, recv, ss, rs):
         copies = []
+
+        def give_half(n):
+            send[n] = total[theirs, n * cut : (n + 1) * cut].astype(bf)
+            copy = to_partner(send.at[n], recv.at[n], ss.at[n], rs.at[n])
+            copy.start()
+            copies.append(copy)
+
         for n in range(n_cut):
             cols = slice(n * cut, (n + 1) * cut)
             total[:, cols] = dot(left, weights[:, cols])
-            send[n] = total[theirs, cols].astype(bf)
-            copy = to_partner(send.at[n], recv.at[n], ss.at[n], rs.at[n])
-            copy.start()
-            copies.append(copy)
+            if n >= AHEAD:
+                give_half(n - AHEAD)
+        for n in range(n_cut - AHEAD, n_cut):
+            give_half(n)
         return copies
 
     wf = w_out_buf[...].astype(f32)
@@ -477,25 +519,34 @@
     w_copies = halves_to_partner((wf * wgain[...].reshape(1, sw)).astype(bf), vow, total_w, wc_send, wc_recv, wc_ss, wc_rs)
     ph("r_takeo")
 
-    def take_o(k, carry):
+    for i in range(heads):
         pltpu.make_async_remote_copy(
-            src_ref=o_send.at[0], dst_ref=o_recv.at[k // 2, lax.rem(k, 2)], send_sem=o_ss.at[0],
-            recv_sem=o_rs.at[k // 2, lax.rem(k, 2)], device_id={"sp": s, "tp": other}, device_id_type=MESH,
+            src_ref=o_send.at[0], dst_ref=o_recv.at[i], send_sem=o_ss.at[0],
+            recv_sem=o_rs.at[i], device_id=partner, device_id_type=MESH,
         ).wait_recv()
-        return carry
-
-    lax.fori_loop(0, 2 * heads, take_o, 0, unroll=True)
     ph("s_sout")
     for j in range(heads // 2):
-        for u in range(2):
-            one = o_recv[2 * j, u].astype(f32)
-            two_ = o_recv[2 * j + 1, u].astype(f32)
-            s_out_buf[u * half : u * half + quarter, 2 * j * hd : 2 * (j + 1) * hd] = jnp.concatenate(
-                [one[:, :hd], two_[:, :hd]], axis=1
-            )
-            s_out_buf[u * half + quarter : (u + 1) * half, 2 * j * hd : 2 * (j + 1) * hd] = jnp.concatenate(
-                [one[:, hd:], two_[:, hd:]], axis=1
-            )
+        one = o_recv[2 * j].astype(f32)
+        two_ = o_recv[2 * j + 1].astype(f32)
+        cols = slice(2 * j * hd, 2 * (j + 1) * hd)
+        s_out_buf[:half, cols] = jnp.concatenate([one[:, :hd], two_[:, :hd]], axis=1)
+        s_out_buf[half:, cols] = jnp.concatenate([one[:, hd:], two_[:, hd:]], axis=1)
+
+    @pl.when(upper)
+    def _():
+        in_late = (lax.broadcasted_iota(jnp.int32, (rows, 2 * hd), 1) // hd) == lax.rem(t + 1, 2)
+        for j in range(heads // 2):
+            pltpu.make_async_remote_copy(
+                src_ref=late_send.at[0], dst_ref=late_recv.at[j], send_sem=late_ss.at[0],
+                recv_sem=late_rs.at[j], device_id=partner, device_id_type=MESH,
+            ).wait_recv()
+            cols = slice(2 * j * hd, 2 * (j + 1) * hd)
+            early = s_out_buf[:, cols]
+            value = late_recv[j].astype(f32)
+            swapped = jnp.concatenate([value[:, hd:], value[:, :hd]], axis=1)
+            joined = (value + swapped * early).astype(bf).astype(f32)
+            s_out_buf[:, cols] = jnp.where(in_late, joined, early)
+
     sf = s_out_buf[...]
     sq_s = squares_to_partner(1, sf * sf)
     ph("t_os")
@@ -512,45 +563,40 @@
 
     ph("w_drain")
     x_copy.wait_send()
-    b_copy.wait_send()
-
-    def scatter_done(k, carry):
-        i = k // 2
-        u = lax.rem(k, 2)
-        chip = 2 * i + t
-
-        @pl.when(jnp.logical_not(jnp.logical_and(chip == s, u == t)))
+
+    for i in range(heads):
+        @pl.when(i != slot)
         def _():
-            pltpu.make_async_remote_copy(
-                src_ref=kv_send.at[i, u], dst_ref=kv_all.at[s, u], send_sem=kv_ss.at[i, u],
-                recv_sem=kv_rs.at[s], device_id={"sp": chip, "tp": u}, device_id_type=MESH,
-            ).wait_send()
-
-        return carry
-
-    lax.fori_loop(0, 2 * heads, scatter_done, 0)
-
-    def forward_sent(k, carry):
-        to_partner(kv_all.at[k, t, :half], kv_all.at[k, t, :half], f_ss.at[k], f_rs.at[k]).wait_send()
-        return carry
-
-    lax.fori_loop(0, n_sp, forward_sent, 0)
+            near_copy(i).wait_send()
+
+    @pl.when(lower)
+    def _():
+        for m in range(heads // 2):
+            far_copy(m, keys_part).wait_send()
+
+    @pl.when(upper)
+    def _():
+        for m in range(heads // 2):
+            far_copy(m, queries_part).wait_send()
 
     @pl.when(s < n_sp - 1)
     def _():
         prev_copy(s + 1).wait_send()
 
-    def gave(k, carry):
-        @pl.when(jnp.logical_not(jnp.logical_and(k == s, t == owner)))
+    gives_low = lower
+    gives_high = jnp.logical_or(jnp.logical_and(upper, above), jnp.logical_and(lower, below))
+    for k in range(n_sp):
+        @pl.when(jnp.logical_and(gives_low if k < heads else gives_high, k != s))
         def _():
-            pltpu.make_async_remote_copy(
-                src_ref=o_send.at[k], dst_ref=o_recv.at[slot, t], send_sem=o_ss.at[k],
-                recv_sem=o_rs.at[slot, t], device_id={"sp": k, "tp": owner}, device_id_type=MESH,
-            ).wait_send()
-
-        return carry
-
-    lax.fori_loop(0, n_sp, gave, 0)
+            o_copy(k).wait_send()
+
+    @pl.when(jnp.logical_and(upper, below))
+    def _():
+        for j in range(heads):
+            @pl.when(j != slot)
+            def _():
+                late_copy(j).wait_send()
+
     sq_w.wait_send()
     sq_s.wait_send()
 
@@ -586,8 +632,7 @@
     sw = wqs.shape[1]
     wide = 2 * hd
     kvw_cols = wkw.shape[1] + wvw.shape[1]
-    n_chunks = n_sp // 4
-    assert 2 * heads == n_sp and rows == WINDOW
+    assert 2 * heads == n_sp and rows == WINDOW and heads == 4 * TILE_BLOCKS
     v = pltpu.VMEM
     dma = pltpu.SemaphoreType.DMA
     anywhere = pl.BlockSpec(memory_space=pl.ANY)
@@ -597,19 +642,20 @@
     scratch = [
         v(pre_gain.shape, f32), pltpu.SMEM(bias.shape, f32), pltpu.SMEM(sinks.shape, f32),
         v(sgain.shape, f32), v(wgain.shape, f32), v(post_gain.shape, f32),
-        v((2, rows, feat_half), bf), v((2, heads, 128), f32), v((2, rows, feat_half), bf),
+        v((2, rows, feat_half), bf), v((2, rows, feat_half), bf),
         split(wqs), split(wks), split(wvs), split(wqw), split(wkw), split(wvw), v(wos.shape, bf), v(wow.shape, bf),
         v((3, rows, sw), f32),
-        v((heads, 2, half + half // 2, wide), bf), v((n_sp, 2, half + half // 2, wide), bf),
-        v((n_sp * half, wide), bf),
-        v((2 * n_chunks, 2 * n_chunks, rows, wide), f32), v((2 * n_chunks, 2 * n_chunks, rows, wide), f32),
+        v((heads, rows + half, wide), bf), v((n_sp, rows + half, wide), bf),
+        v((n_sp * rows, wide), bf),
+        v((n_sp * rows, wide), f32), v((n_sp * rows, wide), f32),
         v((rows, sw), bf), v((rows, kvw_cols), bf), v((rows, kvw_cols), bf), v((rows, sw), bf),
-        v((n_sp, half // 2, wide), bf), v((heads, 2, half // 2, wide), bf), v((rows, sw), f32),
+        v((n_sp, half, wide), bf), v((heads, half, wide), bf),
+        v((heads, rows, wide), bf), v((heads // 2, rows, wide), bf), v((rows, sw), f32),
         v((2, rows, 128), f32), v((2, half, 128), f32), v((rows, feats), f32), v((rows, feats), f32),
         v((n_cut, half, feats // n_cut), bf), v((n_cut, half, feats // n_cut), bf),
         v((n_cut, half, feats // n_cut), bf), v((n_cut, half, feats // n_cut), bf),
-        dma((14,)), dma((6,)), dma, dma, dma, dma, dma, dma((heads, 2)), dma((n_sp,)),
-        dma((n_sp,)), dma((n_sp,)), dma, dma, dma((n_sp,)), dma((heads, 2)), dma((2,)), dma((2,)),
+        dma((14,)), dma((6,)), dma, dma, dma, dma((heads,)), dma((n_sp,)), dma((heads // 2,)),
+        dma, dma, dma((n_sp,)), dma((heads,)), dma((heads,)), dma((heads // 2,)), dma((2,)), dma((2,)),
         dma((n_cut,)), dma((n_cut,)), dma((n_cut,)), dma((n_cut,)), pltpu.SemaphoreType.REGULAR, pltpu.SemaphoreType.REGULAR,
     ]
     return pl.pallas_call(
@@ -803,7 +849,7 @@
 
     def shards(*args):
         heads = args[2].shape[1] // HEAD_DIM
-        if n_tp == 2 and n_tp * heads == n_sp and args[0].shape[0] == WINDOW and n_sp % 4 == 0:
+        if n_tp == 2 and n_tp * heads == n_sp and args[0].shape[0] == WINDOW and heads == 4 * TILE_BLOCKS:
             return one_kernel(n_sp, *args)
         return by_collectives(*args)
 

time: 30.5 us -> 26.6 us (0.87)
  the two profiles are of different devices: /device:TPU:0 before, /device:TPU:21 now
where the time goes in v4:
time: 26.6 us; the launch traced here: 26.4 us
  Pallas kernels  25.7 us (97%)
  local copies, waits for them, and re-layouts  0.71 us (3%)
    pallas_call x1, Pallas kernels, one_kernel(): pl.pallas_call(functools.partial(kernel, n_sp), out_shape=pltpu.VMEM((hal...  25.7 us
    unnamed x1, local copies, waits for them, and re-layouts  0.71 us

profile of v4, /device:TPU:21, one launch (start us, length us, event | category | flops | bytes accessed | tf_op | source)
XLA Modules:
  0.0 26.4 jit_solution(16502175588469528197)
XLA Ops:
  0.0 25.7 %layer.1 = bf16[64,2048]{1,0:T(8,128)(2,1)S(1)} custom-call(bf16[128,1024]{1,0:T(8,128)(2,1)} %tokens.1, f32[2048]{0:T(1024)} %pre_gain_in.1, bf16[2048,512]{1,0:T(8,128)(2,1)} %wqs.1, bf16[2048,512]{1,0:T(8,128)(2,1)} %wks.1, bf16[2048,512]{1,0:T(8,128)(2,1)} %wvs.1, bf16[2048,512]{1,0:T(8,128)(2,1)} %wqw.1, bf16[2048,256]{1,0:T(8,128)(2,1)} %wkw.1, ...), custom_call_target="tpu_custom_call" | custom-call | tf_op jit(solution)/shard_map/layer/pallas_call | solution.py:661
  25.7 0.7 %copy.17 = bf16[64,2048]{1,0:T(8,128)(2,1)} copy(bf16[64,2048]{1,0:T(8,128)(2,1)S(1)} %layer.1) | data formatting | bytes 524288

commit v5 on v4

--- a/solution.py
+++ b/solution.py
@@ -37,9 +37,9 @@
 
 
 TILE_BLOCKS = 2
-AHEAD = 4
-OWN_LAST = 1
-PREV_AT = 1
+AHEAD = 2
+OWN_LAST = 0
+PREV_AT = -1
 UP_AT = 0
 DOWN_AT = 0
 HLB_FIRST = False
@@ -51,7 +51,7 @@
     post_gain_in, out,
     pre_gain, bias, sinks, sgain, wgain, post_gain, x, xg, vqs, vks, vvs, vqw, vkw, vvw, vos, vow,
     proj, kv_send, kv_all, q_pad, acc, mass,
-    qw, kvw, kvw_prev, w_out_buf, o_send, o_recv, late_send, late_recv, s_out_buf,
+    qw, kvw, kvw_prev, w_out_buf, o_send, o_recv, late_send, late_recv, late_scale, s_out_buf,
     sq_send, sq_recv, total_w, comb, c_send, c_recv, wc_send, wc_recv,
     w_sem, small_sem, tok_sem, x_ss, x_rs, kv_ss, kv_rs, far_ss,
     p_ss, p_rs, o_ss, o_rs, late_ss, late_rs, sq_ss, sq_rs, c_ss, c_rs, wc_ss, wc_rs, hello, all_in,
@@ -394,6 +394,15 @@
         for b in range(blocks_in_zone):
             take_q(blocks_in_zone * c + b)
 
+    if PREV_AT < 0:
+        for b in range(blocks_in_zone if PREV_AT == -1 else heads):
+            i = b + (plane * blocks_in_zone if PREV_AT == -1 else 0)
+
+            @pl.when(i != slot)
+            def _():
+                near_copy(i).wait_send()
+
+        send_prev()
     ph("l_arrive0")
     arrive(own_zone)
     send_far(2)
@@ -517,6 +526,28 @@
     sq_w = squares_to_partner(0, wf * wf)
     l_ow.wait()
     w_copies = halves_to_partner((wf * wgain[...].reshape(1, sw)).astype(bf), vow, total_w, wc_send, wc_recv, wc_ss, wc_rs)
+    ph("q_late")
+
+    @pl.when(lower)
+    def _():
+        s_out_buf[...] = jnp.zeros_like(s_out_buf)
+        late_scale[...] = jnp.ones_like(late_scale)
+
+    @pl.when(upper)
+    def _():
+        in_late = (lax.broadcasted_iota(jnp.int32, (rows, 2 * hd), 1) // hd) == lax.rem(t + 1, 2)
+        for j in range(heads // 2):
+            pltpu.make_async_remote_copy(
+                src_ref=late_send.at[0], dst_ref=late_recv.at[j], send_sem=late_ss.at[0],
+                recv_sem=late_rs.at[j], device_id=partner, device_id_type=MESH,
+            ).wait_recv()
+        for j in range(heads // 2):
+            cols = slice(2 * j * hd, 2 * (j + 1) * hd)
+            value = late_recv[j].astype(f32)
+            swapped = jnp.concatenate([value[:, hd:], value[:, :hd]], axis=1)
+            s_out_buf[:, cols] = jnp.where(in_late, value, 0.0)
+            late_scale[:, cols] = jnp.where(in_late, swapped, 1.0)
+
     ph("r_takeo")
 
     for i in range(heads):
@@ -529,23 +560,14 @@
         one = o_recv[2 * j].astype(f32)
         two_ = o_recv[2 * j + 1].astype(f32)
         cols = slice(2 * j * hd, 2 * (j + 1) * hd)
-        s_out_buf[:half, cols] = jnp.concatenate([one[:, :hd], two_[:, :hd]], axis=1)
-        s_out_buf[half:, cols] = jnp.concatenate([one[:, hd:], two_[:, hd:]], axis=1)
-
-    @pl.when(upper)
-    def _():
-        in_late = (lax.broadcasted_iota(jnp.int32, (rows, 2 * hd), 1) // hd) == lax.rem(t + 1, 2)
-        for j in range(heads // 2):
-            pltpu.make_async_remote_copy(
-                src_ref=late_send.at[0], dst_ref=late_recv.at[j], send_sem=late_ss.at[0],
-                recv_sem=late_rs.at[j], device_id=partner, device_id_type=MESH,
-            ).wait_recv()
-            cols = slice(2 * j * hd, 2 * (j + 1) * hd)
-            early = s_out_buf[:, cols]
-            value = late_recv[j].astype(f32)
-            swapped = jnp.concatenate([value[:, hd:], value[:, :hd]], axis=1)
-            joined = (value + swapped * early).astype(bf).astype(f32)
-            s_out_buf[:, cols] = jnp.where(in_late, joined, early)
+        pair = jnp.concatenate(
+            [
+                jnp.concatenate([one[:, :hd], two_[:, :hd]], axis=1),
+                jnp.concatenate([one[:, hd:], two_[:, hd:]], axis=1),
+            ],
+            axis=0,
+        )
+        s_out_buf[:, cols] = (s_out_buf[:, cols] + late_scale[:, cols] * pair).astype(bf).astype(f32)
 
     sf = s_out_buf[...]
     sq_s = squares_to_partner(1, sf * sf)
@@ -564,7 +586,9 @@
     ph("w_drain")
     x_copy.wait_send()
 
-    for i in range(heads):
+    for b in range(heads if PREV_AT >= 0 else blocks_in_zone if PREV_AT == -1 else 0):
+        i = b if PREV_AT >= 0 else b + (1 - plane) * blocks_in_zone
+
         @pl.when(i != slot)
         def _():
             near_copy(i).wait_send()
@@ -650,7 +674,7 @@
         v((n_sp * rows, wide), f32), v((n_sp * rows, wide), f32),
         v((rows, sw), bf), v((rows, kvw_cols), bf), v((rows, kvw_cols), bf), v((rows, sw), bf),
         v((n_sp, half, wide), bf), v((heads, half, wide), bf),
-        v((heads, rows, wide), bf), v((heads // 2, rows, wide), bf), v((rows, sw), f32),
+        v((heads, rows, wide), bf), v((heads // 2, rows, wide), bf), v((rows, sw), f32), v((rows, sw), f32),
         v((2, rows, 128), f32), v((2, half, 128), f32), v((rows, feats), f32), v((rows, feats), f32),
         v((n_cut, half, feats // n_cut), bf), v((n_cut, half, feats // n_cut), bf),
         v((n_cut, half, feats // n_cut), bf), v((n_cut, half, feats // n_cut), bf),

time: 26.6 us -> 26.1 us (0.981)
  the two profiles are of different devices: /device:TPU:21 before, /device:TPU:19 now
where the time goes in v5:
time: 26.1 us; the launch traced here: 25.9 us
  Pallas kernels  25.2 us (97%)
  local copies, waits for them, and re-layouts  0.71 us (3%)
    pallas_call x1, Pallas kernels, one_kernel(): pl.pallas_call(functools.partial(kernel, n_sp), out_shape=pltpu.VMEM((hal...  25.2 us
    unnamed x1, local copies, waits for them, and re-layouts  0.71 us

profile of v5, /device:TPU:19, one launch (start us, length us, event | category | flops | bytes accessed | tf_op | source)
XLA Modules:
  0.0 25.9 jit_solution(15181009892950204509)
XLA Ops:
  0.0 25.2 %layer.1 = bf16[64,2048]{1,0:T(8,128)(2,1)S(1)} custom-call(bf16[128,1024]{1,0:T(8,128)(2,1)} %tokens.1, f32[2048]{0:T(1024)} %pre_gain_in.1, bf16[2048,512]{1,0:T(8,128)(2,1)} %wqs.1, bf16[2048,512]{1,0:T(8,128)(2,1)} %wks.1, bf16[2048,512]{1,0:T(8,128)(2,1)} %wvs.1, bf16[2048,512]{1,0:T(8,128)(2,1)} %wqw.1, bf16[2048,256]{1,0:T(8,128)(2,1)} %wkw.1, ...), custom_call_target="tpu_custom_call" | custom-call | tf_op jit(solution)/shard_map/layer/pallas_call | solution.py:685
  25.2 0.7 %copy.17 = bf16[64,2048]{1,0:T(8,128)(2,1)} copy(bf16[64,2048]{1,0:T(8,128)(2,1)S(1)} %layer.1) | data formatting | bytes 524288
